TPU v7x, 256 devices: a whole 4x4x8 slice. The times are simulated.
256 devices in a mesh: kv: 32 (over z, y), tp: 8 (over x, core).
Axes of the slice: x: 4, y: 4, z: 8, core: 2. Of those that a mesh axis runs over, the one named last changes fastest.
Arguments:
- tokens: bfloat16 [32768, 1024], P('kv', 'tp'), may hold values from -6 to 6
- query_weight: bfloat16 [1024, 2048], P(None, 'tp'), may hold values from -0.1875 to 0.1875
- latent_weight: bfloat16 [1024, 128], replicated, may hold values from -0.1875 to 0.1875
- query_gain: float32 [128], replicated, may hold values from 0.5 to 1.5
- key_gain: float32 [128], replicated, may hold values from 0.5 to 1.5
- value_up: bfloat16 [16, 128, 64], P('tp'), may hold values from -0.5 to 0.5
- out_weight: bfloat16 [1024, 1024], P('tp'), may hold values from -0.25 to 0.25
- out_gain: float32 [1024], replicated, may hold values from 0.5 to 1.5
- chosen: int32 [256, 32], P('kv'), may hold values from -1 to 255, as said below
Outputs:
- mixed_out: bfloat16 [32768, 1024], P('kv', 'tp')
Inputs may be any that keep to these rules, and one draw needn't show every extreme that they name: Row b lists the key blocks chosen for query block b: entry 0 is b itself, then distinct blocks before b, then -1 in every unused place. Block j is held by index j // 8 of kv. All query blocks of one index of kv together choose at most 2 distinct blocks held by any one other index, and some pair of indices reaches that bound; blocks held by the same index are chosen freely.
All inputs are finite; a program needn't handle non-finite values.
Results may differ from a plain program's by a relative error of at most 0.02.
Values may be sent and summed in bfloat16 or wider, within the bound.
No kernel may reach another device: no remote copies, remote signals or barrier semaphores. Data moves between devices by JAX's collectives and lax.ppermute only.
A program may use at most 64 MiB of HBM per device.

v0:
```python
import math

import jax
import jax.numpy as jnp
from jax import lax
from jax.experimental import pallas as pl
from jax.experimental.pallas import tpu as pltpu
from jax.sharding import Mesh
from jax.sharding import PartitionSpec as P


BLOCK = 128
PER_OWNER = 2
KV = ("kv_0", "kv_1")
TP = ("x", "core")
CHIPS = 4
CORES = 2
ROWS = 512

SHIFTS = [(0, 0), (0, 1), (1, 0), (1, 1), (3, 0), (3, 1), (2, 0), (2, 1)]


epsilon = 1e-06
f32 = jnp.float32
bf16 = jnp.bfloat16
i32 = jnp.int32

VMEM = pl.BlockSpec(memory_space=pltpu.VMEM)
SMEM = pl.BlockSpec(memory_space=pltpu.SMEM)


def place(shift, sign):
    dx, dc = shift
    x, core = lax.axis_index("x"), lax.axis_index("core")
    other = core if dc == 0 else 1 - core
    return CORES * lax.rem(x + sign * dx + CHIPS, CHIPS) + other


def moved(part, shift):
    dx, dc = shift
    if shift == (0, 0):
        return part
    pairs = [
        (CORES * x + c, CORES * ((x + dx) % CHIPS) + (c ^ dc))
        for x in range(CHIPS)
        for c in range(CORES)
    ]
    return lax.ppermute(part, TP, pairs)


def gathered(part):
    along_x = {0: part}
    for dx in (1, 3, 2):
        along_x[dx] = moved(part, (dx, 0))
    return [moved(along_x[dx], (0, dc)) for dx, dc in SHIFTS]


def normed(values, gain_row):
    wide = values.astype(f32)
    mean_sq = jnp.mean(wide * wide, axis=-1, keepdims=True)
    return (wide * lax.rsqrt(mean_sq + epsilon) * gain_row).astype(bf16)


def side_by_side(ref):
    return jnp.concatenate([ref[i] for i in range(ref.shape[0])], axis=1)


def prepare_kernel(tokens, chosen, *outs):
    bufs, (wanted, table, count) = outs[:-3], outs[-3:]
    tp = len(bufs)
    blocks = tokens.shape[0] // BLOCK
    sl = BLOCK // tp
    owners = wanted.shape[0]
    for buf, shift in zip(bufs, SHIFTS):
        dest = place(shift, 1)
        buf[0] = tokens[pl.ds(pl.multiple_of(dest * BLOCK, BLOCK), BLOCK), :]
        for b in range(blocks):
            at = pl.multiple_of(b * BLOCK + dest * sl, sl)
            buf[1, b * sl : (b + 1) * sl, :] = tokens[pl.ds(at, sl), :]
    mine = lax.axis_index(KV[0]) * lax.axis_size(KV[1]) + lax.axis_index(KV[1])
    c = chosen[...]
    valid = c >= 0
    owner = lax.shift_right_arithmetic(c, blocks.bit_length() - 1)
    local = c & (blocks - 1)
    lowest = jnp.zeros_like(c)
    lane = lax.broadcasted_iota(i32, (1, wanted.shape[2]), 1)
    for o in range(owners):
        hit = owner == o
        low = jnp.min(jnp.where(hit, local, blocks - 1), keepdims=True)
        high = jnp.max(jnp.where(hit, local, 0), keepdims=True)
        wanted[o] = jnp.where(lane == 0, low, high)
        lowest = jnp.where(hit, low, lowest)
    far = blocks + owner * PER_OWNER + jnp.where(local == lowest, 0, 1)
    table[...] = jnp.where(valid, jnp.where(owner == mine, local, far), 0)
    count[...] = jnp.broadcast_to(
        jnp.sum(jnp.where(valid, 1.0, 0.0), axis=1, keepdims=True).astype(i32), count.shape
    )


def latent_kernel(asked, lw, *refs):
    toks, (lat_out, send_out, tok) = refs[:-3], refs[-3:]
    for part, shift in zip(toks, SHIFTS):
        tok[place(shift, -1)] = part[1]
    lat = jnp.dot(side_by_side(tok), lw[...], preferred_element_type=f32).astype(bf16)
    lat_out[...] = lat.reshape(lat_out.shape)
    for o in range(send_out.shape[0]):
        for s in range(PER_OWNER):
            send_out[o, s] = lat_out[asked[o, 0, s]]


def pick_kernel(table, own, got, *refs):
    outs, pool = refs[:-1], refs[-1]
    blocks = own.shape[0]
    pool[:blocks] = own[...]
    pool[blocks:] = got[...]
    for out, shift in zip(outs, SHIFTS):
        dest = place(shift, 1)
        for c in range(out.shape[0]):
            out[c] = pool[table[dest, c]]


def query_kernel(gain, *refs):
    out, tok = refs[-2:]
    n = len(SHIFTS)
    toks, pieces = refs[:n], refs[n:-2]
    for part, shift in zip(toks, SHIFTS):
        tok[place(shift, -1)] = part[0]
    lhs = side_by_side(tok)
    width = gain.shape[1]
    at = 0
    for piece in pieces:
        acc = jnp.dot(lhs, piece[...], preferred_element_type=f32).astype(bf16)
        for h in range(acc.shape[1] // width):
            out[at] = normed(acc[:, h * width : (h + 1) * width], gain[...])
            at += 1


def add_piece(q_ref, kv, kgain, count, src, acc_in, acc):
    picks, sl, width = kv.shape
    keys = picks * sl
    per = ROWS // BLOCK
    lat = kv[...].reshape(keys, width)
    on = lax.broadcasted_iota(i32, (keys, width), 0) < count * sl
    lat = jnp.where(on, lat, jnp.zeros_like(lat))
    ones = jnp.where(on, jnp.ones_like(lat), jnp.zeros_like(lat))
    k = normed(lat, kgain[...] * (width**-0.5 * math.log2(math.e)))
    v = jnp.concatenate([lat, ones], axis=1)
    at = lax.broadcasted_iota(i32, (ROWS, BLOCK), 1)
    row = lax.broadcasted_iota(i32, (ROWS, BLOCK), 0) & (BLOCK - 1)
    for r in range(q_ref.shape[0] // per):
        q = jnp.concatenate([q_ref[r * per + h] for h in range(per)], axis=0)
        s = lax.dot_general(q, k, (((1,), (1,)), ((), ())), preferred_element_type=f32)
        w = jnp.exp2(s)
        own = jnp.where((at >= sl) | (at + src * sl <= row), w[:, :BLOCK], 0.0)
        w = jnp.concatenate([own, w[:, BLOCK:]], axis=1).astype(bf16)
        got = jnp.dot(w, v, preferred_element_type=f32)
        acc[r] = got if acc_in is None else acc_in[r] + got


def attend_kernel(shifts, first, last, count, q_ref, kgain, *refs):
    n = len(shifts)
    pieces, rest = refs[:n], refs[n:]
    acc_in, rest = (None, rest) if first else (rest[0], rest[1:])
    acc = rest[-1]
    here = count[place((0, 0), 1), 0]
    for piece, shift in zip(pieces, shifts):
        add_piece(q_ref, piece, kgain, here, place(shift, -1), acc_in, acc)
        acc_in = acc
    if last:
        out = rest[0]
        width = out.shape[2]
        per = ROWS // BLOCK
        for r in range(out.shape[0] // per):
            res = (acc[r, :, :width] / acc[r, :, width:]).astype(bf16)
            out[r * per : (r + 1) * per] = res.reshape(per, BLOCK, width)


def output_kernel(*refs):
    pieces, (att, gain, out) = refs[:-3], refs[-3:]
    model = gain.shape[1]
    sides = []
    for i, piece in enumerate(pieces):
        up = piece[:, model:]
        low = jnp.dot(att[2 * i], up, preferred_element_type=f32)
        high = jnp.dot(att[2 * i + 1], up, preferred_element_type=f32)
        lane = lax.broadcasted_iota(i32, low.shape, 1)
        sides.append(jnp.where(lane < up.shape[1] // 2, low, high).astype(bf16))
    lhs = jnp.concatenate(sides, axis=1)
    rhs = jnp.concatenate([p[:, :model] for p in pieces], axis=0)
    acc = jnp.dot(lhs, rhs, preferred_element_type=f32)
    mean_sq = jnp.mean(acc * acc, axis=-1, keepdims=True)
    res = (acc * lax.rsqrt(mean_sq + epsilon) * gain[...]).astype(bf16)
    w = out.shape[2]
    for p in range(out.shape[0]):
        out[p] = res[:, p * w : (p + 1) * w]


def shape(dims, kind=bf16):
    return jax.ShapeDtypeStruct(dims, kind)


def shards(
    tokens,
    query_weight,
    latent_weight,
    query_gain,
    key_gain,
    value_up,
    out_weight,
    out_gain,
    chosen,
):
    rows, feats = tokens.shape
    lat_w = latent_weight.shape[1]
    blocks = rows // BLOCK
    picks = chosen.shape[1]
    owners = lax.axis_size(KV)
    tp = len(SHIFTS)
    sl = BLOCK // tp
    heads = query_weight.shape[1] // lat_w * tp

    *bufs, wanted, table, count = pl.pallas_call(
        prepare_kernel,
        out_shape=[shape((2, BLOCK, feats))] * tp
        + [shape((owners, 1, BLOCK), i32), shape((blocks, picks), i32), shape((blocks, BLOCK), i32)],
        in_specs=[VMEM, VMEM],
        out_specs=[VMEM] * (tp + 3),
        name="prepare",
    )(tokens, chosen)

    toks = [moved(b, s) for b, s in zip(bufs, SHIFTS)]
    asked = lax.all_to_all(wanted, KV, split_axis=0, concat_axis=0, tiled=True)

    query_parts = gathered(query_weight)

    latent, send = pl.pallas_call(
        latent_kernel,
        out_shape=(shape((blocks, sl, lat_w)), shape((owners, PER_OWNER, sl, lat_w))),
        in_specs=[SMEM] + [VMEM] * (tp + 1),
        out_specs=(VMEM, VMEM),
        scratch_shapes=[pltpu.VMEM((tp, BLOCK, feats), bf16)],
        name="latent",
    )(asked, latent_weight, *toks)

    got = lax.all_to_all(send, KV, split_axis=0, concat_axis=0, tiled=True)
    got = got.reshape(owners * PER_OWNER, sl, lat_w)

    picked = pl.pallas_call(
        pick_kernel,
        out_shape=[shape((picks, sl, lat_w))] * tp,
        in_specs=[SMEM, VMEM, VMEM],
        out_specs=[VMEM] * tp,
        scratch_shapes=[pltpu.VMEM((blocks + owners * PER_OWNER, sl, lat_w), bf16)],
        name="pick",
    )(table, latent, got)
    kv = {}
    for part, s in zip(picked, SHIFTS):
        kv[s] = moved(part, s)

    up = value_up.swapaxes(0, 1).reshape(lat_w, -1)
    weight_parts = gathered(jnp.concatenate([out_weight, up], axis=1))

    q = pl.pallas_call(
        query_kernel,
        out_shape=shape((heads, BLOCK, lat_w)),
        in_specs=[VMEM] * (2 * tp + 1),
        out_specs=VMEM,
        scratch_shapes=[pltpu.VMEM((tp, BLOCK, feats), bf16)],
        name="query",
    )(query_gain[None, :], *toks, *query_parts)

    sums = (heads * BLOCK // ROWS, ROWS, 2 * lat_w)
    state = []
    for shifts in (SHIFTS[:2], SHIFTS[2:6], SHIFTS[6:]):
        first, last = shifts[0] == SHIFTS[0], shifts[-1] == SHIFTS[-1]

        def kernel(*refs, shifts=shifts, first=first, last=last):
            attend_kernel(shifts, first, last, *refs)

        state = [
            pl.pallas_call(
                kernel,
                out_shape=shape((heads, BLOCK, lat_w)) if last else shape(sums, f32),
                in_specs=[SMEM] + [VMEM] * (2 + len(shifts) + len(state)),
                out_specs=VMEM,
                scratch_shapes=[pltpu.VMEM(sums, f32)] if last else [],
            )(count, q, key_gain[None, :], *[kv[s] for s in shifts], *state)
        ]

    width = out_weight.shape[1] // tp
    res = pl.pallas_call(
        output_kernel,
        out_shape=shape((tp, BLOCK, width)),
        in_specs=[VMEM] * (tp + 2),
        out_specs=VMEM,
        name="output",
    )(*weight_parts, state[0], out_gain[None, :])
    res = lax.all_to_all(res, TP, split_axis=0, concat_axis=0, tiled=True)
    return res.reshape(rows, width)


def solution(mesh):
    torus = Mesh(mesh.devices.reshape(8, CHIPS, 4, CORES), ("kv_0", "kv_1", "x", "core"))
    in_specs = (
        P(KV, TP),
        P(None, TP),
        P(),
        P(),
        P(),
        P(TP, None, None),
        P(TP, None),
        P(),
        P(KV, None),
    )
    return jax.shard_map(
        shards, mesh=torus, in_specs=in_specs, out_specs=P(KV, TP), check_vma=False
    )
```

profile of v0, /device:TPU:8, one launch (start us, length us, event | category | flops | bytes accessed | tf_op | source)
XLA Modules:
  0.0 121.5 jit_solution(2776116297194586781)
XLA Ops:
  3.5 2.0 %prepare.1 = (bf16[2,128,128]{2,1,0:T(8,128)(2,1)}, bf16[2,128,128]{2,1,0:T(8,128)(2,1)}, bf16[2,128,128]{2,1,0:T(8,128)(2,1)}, bf16[2,128,128]{2,1,0:T(8,128)(2...) custom-call(bf16[1024,128]{1,0:T(8,128)(2,1)} %tokens.1, ...), custom_call_target="tpu_custom_call" | custom-call | tf_op jit(solution)/shard_map/prepare/pallas_call | solution.py:222
  5.5 1.8 %collective-permute-start.10 = (bf16[2,128,128]{2,1,0:T(8,128)(2,1)}, bf16[2,128,128]{2,1,0:T(8,128)(2,1)S(1)}, u32[]{:S(2)}, u32[]{:S(2)}) collective-permute-start(bf16[2,128,128]{2,1,0:T(8,128)(2,1)} %get-tuple-element.31), channel_id=1, source_target_pairs={{0,6},{1,7},{2,0},{3,1},{4,2},{5,3},{6,4},{7,5},{8,14},{9,15},{10,... | collective-permute-start | bytes 196616 | tf_op jit(solution)/shard_map/ppermute | solution.py:48
  9.1 2.7 %collective-permute-start.13 = (bf16[2,128,128]{2,1,0:T(8,128)(2,1)}, bf16[2,128,128]{2,1,0:T(8,128)(2,1)S(1)}, u32[]{:S(2)}, u32[]{:S(2)}) collective-permute-start(bf16[2,128,128]{2,1,0:T(8,128)(2,1)} %get-tuple-element.34), channel_id=1, source_target_pairs={{0,5},{1,4},{2,7},{3,6},{4,1},{5,0},{6,3},{7,2},{8,13},{9,12},{10,... | collective-permute-start | bytes 196616 | tf_op jit(solution)/shard_map/ppermute | solution.py:48
  12.4 1.7 %collective-permute-done.12.refs_6_ = bf16[2,128,128]{2,1,0:T(8,128)(2,1)S(1)} collective-permute-done((bf16[2,128,128]{2,1,0:T(8,128)(2,1)}, bf16[2,128,128]{2,1,0:T(8,128)(2,1)S(1)}, u32[]{:S(2)}, u32[]{:S(2)}) %collective-permute-start.12) | collective-permute-done | bytes 65568 | tf_op jit(solution)/shard_map/ppermute | solution.py:48
  19.6 11.7 %all-to-all-start = ((s32[32,1,128]{2,1,0:T(1,128)}), s32[32,1,128]{2,1,0:T(1,128)S(1)}, u32[]{:S(2)}, u32[]{:S(2)}) async-start(s32[32,1,128]{2,1,0:T(1,128)} %get-tuple-element.36), calls=%async_computation | async-start | bytes 32768 | tf_op jit(solution)/shard_map/all_to_all | solution.py:232
  32.6 7.3 %all-to-all-done.asked = s32[32,1,128]{2,1,0:T(1,128)S(1)} async-done(((s32[32,1,128]{2,1,0:T(1,128)}), s32[32,1,128]{2,1,0:T(1,128)S(1)}, u32[]{:S(2)}, u32[]{:S(2)}) %all-to-all-start) | async-done | bytes 16416 | tf_op jit(solution)/shard_map/all_to_all | solution.py:232
  40.5 2.1 %latent.1 = (bf16[8,16,128]{2,1,0:T(8,128)(2,1)}, bf16[32,2,16,128]{3,2,1,0:T(8,128)(2,1)}) custom-call(s32[32,1,128]{2,1,0:T(1,128)} %copy-done.22, bf16[1024,128]{1,0:T(8,128)(2,1)} %lw.1, bf16[2,128,128]{2,1,0:T(8,128)(2,1)} %get-tuple-element.27.refs_0_, bf16[2,128,128]{2,1,0:T(8,128)(2,1)} %copy-done.13, bf16[2,128,128]{2,1,0:T(8,128)(2,1)} %copy-done.14, ...), custom_call_target="tpu_custom_call" | custom-call | tf_op jit(solution)/shard_map/latent/pallas_call | solution.py:236
  42.6 5.0 %all-to-all-start.1 = ((bf16[32,2,16,128]{3,2,1,0:T(8,128)(2,1)}), bf16[32,2,16,128]{3,2,1,0:T(8,128)(2,1)S(1)}, u32[]{:S(2)}, u32[]{:S(2)}) async-start(bf16[32,2,16,128]{3,2,1,0:T(8,128)(2,1)} %get-tuple-element.38), calls=%async_computation.1 | async-start | bytes 524288 | tf_op jit(solution)/shard_map/all_to_all | solution.py:245
  47.7 1.9 %collective-permute-start.5 = (bf16[128,1152]{1,0:T(8,128)(2,1)S(1)}, bf16[128,1152]{1,0:T(8,128)(2,1)}, u32[]{:S(2)}, u32[]{:S(2)}) collective-permute-start(bf16[128,1152]{1,0:T(8,128)(2,1)S(1)} %pad_maximum_fusion.refs_0_), channel_id=1, source_target_pairs={{0,4},{1,5},{2,6},{3,7},{4,0},{5,1},{6,2},{7,3},{8,12},{9,13},{10,... | collective-permute-start | bytes 884744 | tf_op jit(solution)/shard_map/ppermute | solution.py:48
  50.1 8.0 %all-to-all-done.1 = bf16[32,2,16,128]{3,2,1,0:T(8,128)(2,1)S(1)} async-done(((bf16[32,2,16,128]{3,2,1,0:T(8,128)(2,1)}), bf16[32,2,16,128]{3,2,1,0:T(8,128)(2,1)S(1)}, u32[]{:S(2)}, u32[]{:S(2)}) %all-to-all-start.1) | async-done | bytes 262176 | tf_op jit(solution)/shard_map/all_to_all | solution.py:245
  58.8 2.1 %pick.1 = (bf16[32,16,128]{2,1,0:T(8,128)(2,1)}, bf16[32,16,128]{2,1,0:T(8,128)(2,1)}, bf16[32,16,128]{2,1,0:T(8,128)(2,1)}, bf16[32,16,128]{2,1,0:T(8,128)(2,1)...) custom-call(s32[8,32]{1,0:T(8,128)} %get-tuple-element.35.table, ...), custom_call_target="tpu_custom_call" | custom-call | tf_op jit(solution)/shard_map/pick/pallas_call | solution.py:248
  62.5 2.0 %collective-permute-start.24 = (bf16[32,16,128]{2,1,0:T(8,128)(2,1)}, bf16[32,16,128]{2,1,0:T(8,128)(2,1)S(1)}, u32[]{:S(2)}, u32[]{:S(2)}) collective-permute-start(bf16[32,16,128]{2,1,0:T(8,128)(2,1)} %get-tuple-element.42), channel_id=1, source_target_pairs={{0,3},{1,2},{2,5},{3,4},{4,7},{5,6},{6,1},{7,0},{8,11},{9,10},{10,... | collective-permute-start | bytes 393224 | tf_op jit(solution)/shard_map/ppermute | solution.py:48
  64.6 4.3 %collective-permute-done.23.refs_3_ = bf16[32,16,128]{2,1,0:T(8,128)(2,1)S(1)} collective-permute-done((bf16[32,16,128]{2,1,0:T(8,128)(2,1)}, bf16[32,16,128]{2,1,0:T(8,128)(2,1)S(1)}, u32[]{:S(2)}, u32[]{:S(2)}) %collective-permute-start.23) | collective-permute-done | bytes 131104 | tf_op jit(solution)/shard_map/ppermute | solution.py:48
  68.9 1.9 %collective-permute-start.25 = (bf16[32,16,128]{2,1,0:T(8,128)(2,1)}, bf16[32,16,128]{2,1,0:T(8,128)(2,1)S(1)}, u32[]{:S(2)}, u32[]{:S(2)}) collective-permute-start(bf16[32,16,128]{2,1,0:T(8,128)(2,1)} %get-tuple-element.43), channel_id=1, source_target_pairs={{0,6},{1,7},{2,0},{3,1},{4,2},{5,3},{6,4},{7,5},{8,14},{9,15},{10,... | collective-permute-start | bytes 393224 | tf_op jit(solution)/shard_map/ppermute | solution.py:48
  72.5 1.6 %collective-permute-done.25.refs_5_ = bf16[32,16,128]{2,1,0:T(8,128)(2,1)S(1)} collective-permute-done((bf16[32,16,128]{2,1,0:T(8,128)(2,1)}, bf16[32,16,128]{2,1,0:T(8,128)(2,1)S(1)}, u32[]{:S(2)}, u32[]{:S(2)}) %collective-permute-start.25) | collective-permute-done | bytes 131104 | tf_op jit(solution)/shard_map/ppermute | solution.py:48
  74.0 2.5 %collective-permute-start.21 = (bf16[32,16,128]{2,1,0:T(8,128)(2,1)}, bf16[32,16,128]{2,1,0:T(8,128)(2,1)S(1)}, u32[]{:S(2)}, u32[]{:S(2)}) collective-permute-start(bf16[32,16,128]{2,1,0:T(8,128)(2,1)} %get-tuple-element.39), channel_id=1, source_target_pairs={{0,4},{1,5},{2,6},{3,7},{4,0},{5,1},{6,2},{7,3},{8,12},{9,13},{10,... | collective-permute-start | bytes 393224 | tf_op jit(solution)/shard_map/ppermute | solution.py:48
  77.8 2.9 %collective-permute-done.21.refs_3_ = bf16[32,16,128]{2,1,0:T(8,128)(2,1)S(1)} collective-permute-done((bf16[32,16,128]{2,1,0:T(8,128)(2,1)}, bf16[32,16,128]{2,1,0:T(8,128)(2,1)S(1)}, u32[]{:S(2)}, u32[]{:S(2)}) %collective-permute-start.21) | collective-permute-done | bytes 131104 | tf_op jit(solution)/shard_map/ppermute | solution.py:48
  81.4 2.8 %collective-permute-start.22 = (bf16[32,16,128]{2,1,0:T(8,128)(2,1)}, bf16[32,16,128]{2,1,0:T(8,128)(2,1)}, u32[]{:S(2)}, u32[]{:S(2)}) collective-permute-start(bf16[32,16,128]{2,1,0:T(8,128)(2,1)} %get-tuple-element.40), channel_id=1, source_target_pairs={{0,5},{1,4},{2,7},{3,6},{4,1},{5,0},{6,3},{7,2},{8,13},{9,12},{10,... | collective-permute-start | bytes 393224 | tf_op jit(solution)/shard_map/ppermute | solution.py:48
  84.2 4.0 %query.1.refs_1_ = bf16[16,128,128]{2,1,0:T(8,128)(2,1)} custom-call(f32[1,128]{1,0:T(1,128)} %bitcast.15, bf16[2,128,128]{2,1,0:T(8,128)(2,1)} %get-tuple-element.27.refs_0_, bf16[2,128,128]{2,1,0:T(8,128)(2,1)} %copy-done.13, bf16[2,128,128]{2,1,0:T(8,128)(2,1)} %copy-done.14, bf16[2,128,128]{2,1,0:T(8,128)(2,1)} %copy-done.15, ...), custom_call_target="tpu_custom_call" | custom-call | tf_op jit(solution)/shard_map/query/pallas_call | solution.py:263
  88.3 5.1 %shard_map.91.refs_7_ = f32[4,512,256]{2,1,0:T(8,128)} custom-call(s32[8,128]{1,0:T(8,128)} %get-tuple-element.26.refs_0_, bf16[16,128,128]{2,1,0:T(8,128)(2,1)} %query.1.refs_1_, f32[1,128]{1,0:T(1,128)} %bitcast.11, bf16[32,16,128]{2,1,0:T(8,128)(2,1)} %get-tuple-element.45.refs_3_, bf16[32,16,128]{2,1,0:T(8,128)(2,1)} %copy-done.16), custom_call_target="tpu_custom_call" | custom-call | tf_op jit(solution)/shard_map/pallas_call | solution.py:281
  93.4 8.1 %shard_map.92.refs_5_ = f32[4,512,256]{2,1,0:T(8,128)} custom-call(s32[8,128]{1,0:T(8,128)} %get-tuple-element.26.refs_0_, bf16[16,128,128]{2,1,0:T(8,128)(2,1)} %query.1.refs_1_, f32[1,128]{1,0:T(1,128)} %bitcast.12, bf16[32,16,128]{2,1,0:T(8,128)(2,1)} %copy-done.17, bf16[32,16,128]{2,1,0:T(8,128)(2,1)} %copy-done.18, bf16[32,16,128]{2,1,0:T(8,128)(2,1)} %copy-done.19, ...), custom_call_target="tpu_custom_call" | custom-call | tf_op jit(solution)/shard_map/pallas_call | solution.py:281
  101.5 5.3 %shard_map.93.refs_8_ = bf16[16,128,128]{2,1,0:T(8,128)(2,1)} custom-call(s32[8,128]{1,0:T(8,128)} %get-tuple-element.26.refs_0_, bf16[16,128,128]{2,1,0:T(8,128)(2,1)} %query.1.refs_1_, f32[1,128]{1,0:T(1,128)} %bitcast.13, bf16[32,16,128]{2,1,0:T(8,128)(2,1)} %copy-done.21, bf16[32,16,128]{2,1,0:T(8,128)(2,1)} %collective-permute-done.22.refs_4_, ...), custom_call_target="tpu_custom_call" | custom-call | tf_op jit(solution)/shard_map/pallas_call | solution.py:281
  106.8 3.2 %output.1 = bf16[8,128,128]{2,1,0:T(8,128)(2,1)} custom-call(bf16[128,1152]{1,0:T(8,128)(2,1)} %copy-done, bf16[128,1152]{1,0:T(8,128)(2,1)} %collective-permute-done.refs_1_, bf16[128,1152]{1,0:T(8,128)(2,1)} %copy-done.8, bf16[128,1152]{1,0:T(8,128)(2,1)} %collective-permute-done.2.refs_3_, bf16[128,1152]{1,0:T(8,128)(2,1)} %collective-permute-done.3.refs_4_, ...), custom_call_target="tpu_custom_call" | custom-call | tf_op jit(solution)/shard_map/output/pallas_call | solution.py:291
  110.0 10.8 %all_to_all.15 = bf16[8,128,128]{2,1,0:T(8,128)(2,1)S(1)} all-to-all(bf16[8,128,128]{2,1,0:T(8,128)(2,1)} %output.1), channel_id=1, replica_groups=mesh['kv_0'=8,'kv_1'=4,'x'=4,'core'=2] {'x','core'}, dimensions={0} | all-to-all | bytes 524288 | tf_op jit(solution)/shard_map/all_to_all | solution.py:298
  (94 shorter events, 20.4 us)
Async XLA Ops:
  1.9 45.6 %collective-permute-start.1 = (bf16[128,1152]{1,0:T(8,128)(2,1)S(1)}, bf16[128,1152]{1,0:T(8,128)(2,1)S(1)}, u32[]{:S(2)}, u32[]{:S(2)}) collective-permute-start(bf16[128,1152]{1,0:T(8,128)(2,1)S(1)} %pad_maximum_fusion.refs_0_), channel_id=1, source_target_pairs={{0,2},{1,3},{2,4},{3,5},{4,6},{5,7},{6,0},{7,1},{8,10},{9,11},{10,... | collective-permute-start | bytes 884744 | tf_op jit(solution)/shard_map/ppermute | solution.py:48
  9.1 6.7 %collective-permute-start.13 = (bf16[2,128,128]{2,1,0:T(8,128)(2,1)}, bf16[2,128,128]{2,1,0:T(8,128)(2,1)S(1)}, u32[]{:S(2)}, u32[]{:S(2)}) collective-permute-start(bf16[2,128,128]{2,1,0:T(8,128)(2,1)} %get-tuple-element.34), channel_id=1, source_target_pairs={{0,5},{1,4},{2,7},{3,6},{4,1},{5,0},{6,3},{7,2},{8,13},{9,12},{10,... | collective-permute-start | bytes 196616 | tf_op jit(solution)/shard_map/ppermute | solution.py:48
  11.8 7.8 %collective-permute-start.8 = (bf16[2,128,128]{2,1,0:T(8,128)(2,1)}, bf16[2,128,128]{2,1,0:T(8,128)(2,1)S(1)}, u32[]{:S(2)}, u32[]{:S(2)}) collective-permute-start(bf16[2,128,128]{2,1,0:T(8,128)(2,1)} %get-tuple-element.29), channel_id=1, source_target_pairs={{0,2},{1,3},{2,4},{3,5},{4,6},{5,7},{6,0},{7,1},{8,10},{9,11},{10,... | collective-permute-start | bytes 196616 | tf_op jit(solution)/shard_map/ppermute | solution.py:48
  14.1 35.5 %collective-permute-start.15 = (bf16[1024,256]{1,0:T(8,128)(2,1)}, bf16[1024,256]{1,0:T(8,128)(2,1)S(1)}, u32[]{:S(2)}, u32[]{:S(2)}) collective-permute-start(bf16[1024,256]{1,0:T(8,128)(2,1)} %refs_8_.1), channel_id=1, source_target_pairs={{0,2},{1,3},{2,4},{3,5},{4,6},{5,7},{6,0},{7,1},{8,10},{9,11},{10,... | collective-permute-start | bytes 1572872 | tf_op jit(solution)/shard_map/ppermute | solution.py:48
  15.8 33.8 %collective-permute-start.17 = (bf16[1024,256]{1,0:T(8,128)(2,1)}, bf16[1024,256]{1,0:T(8,128)(2,1)S(1)}, u32[]{:S(2)}, u32[]{:S(2)}) collective-permute-start(bf16[1024,256]{1,0:T(8,128)(2,1)} %refs_8_.1), channel_id=1, source_target_pairs={{0,6},{1,7},{2,0},{3,1},{4,2},{5,3},{6,4},{7,5},{8,14},{9,15},{10,... | collective-permute-start | bytes 1572872 | tf_op jit(solution)/shard_map/ppermute | solution.py:48
  17.4 30.3 %collective-permute-start.3 = (bf16[128,1152]{1,0:T(8,128)(2,1)S(1)}, bf16[128,1152]{1,0:T(8,128)(2,1)}, u32[]{:S(2)}, u32[]{:S(2)}) collective-permute-start(bf16[128,1152]{1,0:T(8,128)(2,1)S(1)} %pad_maximum_fusion.refs_0_), channel_id=1, source_target_pairs={{0,6},{1,7},{2,0},{3,1},{4,2},{5,3},{6,4},{7,5},{8,14},{9,15},{10,... | collective-permute-start | bytes 884744 | tf_op jit(solution)/shard_map/ppermute | solution.py:48
  19.6 11.7 %collective-permute-start.9 = (bf16[2,128,128]{2,1,0:T(8,128)(2,1)}, bf16[2,128,128]{2,1,0:T(8,128)(2,1)S(1)}, u32[]{:S(2)}, u32[]{:S(2)}) collective-permute-start(bf16[2,128,128]{2,1,0:T(8,128)(2,1)} %get-tuple-element.30), channel_id=1, source_target_pairs={{0,3},{1,2},{2,5},{3,4},{4,7},{5,6},{6,1},{7,0},{8,11},{9,10},{10,... | collective-permute-start | bytes 196616 | tf_op jit(solution)/shard_map/ppermute | solution.py:48
  19.6 20.3 %all-to-all-start = ((s32[32,1,128]{2,1,0:T(1,128)}), s32[32,1,128]{2,1,0:T(1,128)S(1)}, u32[]{:S(2)}, u32[]{:S(2)}) async-start(s32[32,1,128]{2,1,0:T(1,128)} %get-tuple-element.36), calls=%async_computation | async-start | bytes 32768 | tf_op jit(solution)/shard_map/all_to_all | solution.py:232
  31.3 29.7 %collective-permute-start.19 = (bf16[1024,256]{1,0:T(8,128)(2,1)}, bf16[1024,256]{1,0:T(8,128)(2,1)S(1)}, u32[]{:S(2)}, u32[]{:S(2)}) collective-permute-start(bf16[1024,256]{1,0:T(8,128)(2,1)} %refs_8_.1), channel_id=1, source_target_pairs={{0,4},{1,5},{2,6},{3,7},{4,0},{5,1},{6,2},{7,3},{8,12},{9,13},{10,... | collective-permute-start | bytes 1572872 | tf_op jit(solution)/shard_map/ppermute | solution.py:48
  42.6 15.5 %all-to-all-start.1 = ((bf16[32,2,16,128]{3,2,1,0:T(8,128)(2,1)}), bf16[32,2,16,128]{3,2,1,0:T(8,128)(2,1)S(1)}, u32[]{:S(2)}, u32[]{:S(2)}) async-start(bf16[32,2,16,128]{3,2,1,0:T(8,128)(2,1)} %get-tuple-element.38), calls=%async_computation.1 | async-start | bytes 524288 | tf_op jit(solution)/shard_map/all_to_all | solution.py:245
  47.6 14.5 %collective-permute-start.14 = (bf16[1024,256]{1,0:T(8,128)(2,1)S(1)}, bf16[1024,256]{1,0:T(8,128)(2,1)S(1)}, u32[]{:S(2)}, u32[]{:S(2)}) collective-permute-start(bf16[1024,256]{1,0:T(8,128)(2,1)S(1)} %copy-done.2), channel_id=1, source_target_pairs={{0,1},{1,0},{2,3},{3,2},{4,5},{5,4},{6,7},{7,6},{8,9},{9,8},{10,11... | collective-permute-start | bytes 1572872 | tf_op jit(solution)/shard_map/ppermute | solution.py:48
  47.7 13.2 %collective-permute-start.5 = (bf16[128,1152]{1,0:T(8,128)(2,1)S(1)}, bf16[128,1152]{1,0:T(8,128)(2,1)}, u32[]{:S(2)}, u32[]{:S(2)}) collective-permute-start(bf16[128,1152]{1,0:T(8,128)(2,1)S(1)} %pad_maximum_fusion.refs_0_), channel_id=1, source_target_pairs={{0,4},{1,5},{2,6},{3,7},{4,0},{5,1},{6,2},{7,3},{8,12},{9,13},{10,... | collective-permute-start | bytes 884744 | tf_op jit(solution)/shard_map/ppermute | solution.py:48
  49.6 31.2 %collective-permute-start.16 = (bf16[1024,256]{1,0:T(8,128)(2,1)S(1)}, bf16[1024,256]{1,0:T(8,128)(2,1)}, u32[]{:S(2)}, u32[]{:S(2)}) collective-permute-start(bf16[1024,256]{1,0:T(8,128)(2,1)S(1)} %collective-permute-done.15.refs_10_), channel_id=1, source_target_pairs={{0,1},{1,0},{2,3},{3,2},{4,5},{5,4},{6,7},{7,6},{8,9},{9,8},{10,11... | collective-permute-start | bytes 1572872 | tf_op jit(solution)/shard_map/ppermute | solution.py:48
  49.6 31.7 %collective-permute-start.18 = (bf16[1024,256]{1,0:T(8,128)(2,1)S(1)}, bf16[1024,256]{1,0:T(8,128)(2,1)}, u32[]{:S(2)}, u32[]{:S(2)}) collective-permute-start(bf16[1024,256]{1,0:T(8,128)(2,1)S(1)} %collective-permute-done.17.refs_12_), channel_id=1, source_target_pairs={{0,1},{1,0},{2,3},{3,2},{4,5},{5,4},{6,7},{7,6},{8,9},{9,8},{10,11... | collective-permute-start | bytes 1572872 | tf_op jit(solution)/shard_map/ppermute | solution.py:48
  61.0 7.9 %collective-permute-start.23 = (bf16[32,16,128]{2,1,0:T(8,128)(2,1)}, bf16[32,16,128]{2,1,0:T(8,128)(2,1)S(1)}, u32[]{:S(2)}, u32[]{:S(2)}) collective-permute-start(bf16[32,16,128]{2,1,0:T(8,128)(2,1)} %get-tuple-element.41), channel_id=1, source_target_pairs={{0,2},{1,3},{2,4},{3,5},{4,6},{5,7},{6,0},{7,1},{8,10},{9,11},{10,... | collective-permute-start | bytes 393224 | tf_op jit(solution)/shard_map/ppermute | solution.py:48
  62.1 19.2 %collective-permute-start.20 = (bf16[1024,256]{1,0:T(8,128)(2,1)S(1)}, bf16[1024,256]{1,0:T(8,128)(2,1)S(1)}, u32[]{:S(2)}, u32[]{:S(2)}) collective-permute-start(bf16[1024,256]{1,0:T(8,128)(2,1)S(1)} %collective-permute-done.19.refs_14_), channel_id=1, source_target_pairs={{0,1},{1,0},{2,3},{3,2},{4,5},{5,4},{6,7},{7,6},{8,9},{9,8},{10,11... | collective-permute-start | bytes 1572872 | tf_op jit(solution)/shard_map/ppermute | solution.py:48
  62.5 8.4 %collective-permute-start.24 = (bf16[32,16,128]{2,1,0:T(8,128)(2,1)}, bf16[32,16,128]{2,1,0:T(8,128)(2,1)S(1)}, u32[]{:S(2)}, u32[]{:S(2)}) collective-permute-start(bf16[32,16,128]{2,1,0:T(8,128)(2,1)} %get-tuple-element.42), channel_id=1, source_target_pairs={{0,3},{1,2},{2,5},{3,4},{4,7},{5,6},{6,1},{7,0},{8,11},{9,10},{10,... | collective-permute-start | bytes 393224 | tf_op jit(solution)/shard_map/ppermute | solution.py:48
  70.9 6.9 %collective-permute-start.26 = (bf16[32,16,128]{2,1,0:T(8,128)(2,1)}, bf16[32,16,128]{2,1,0:T(8,128)(2,1)S(1)}, u32[]{:S(2)}, u32[]{:S(2)}) collective-permute-start(bf16[32,16,128]{2,1,0:T(8,128)(2,1)} %get-tuple-element.44), channel_id=1, source_target_pairs={{0,7},{1,6},{2,1},{3,0},{4,3},{5,2},{6,5},{7,4},{8,15},{9,14},{10,... | collective-permute-start | bytes 393224 | tf_op jit(solution)/shard_map/ppermute | solution.py:48
  74.0 6.7 %collective-permute-start.21 = (bf16[32,16,128]{2,1,0:T(8,128)(2,1)}, bf16[32,16,128]{2,1,0:T(8,128)(2,1)S(1)}, u32[]{:S(2)}, u32[]{:S(2)}) collective-permute-start(bf16[32,16,128]{2,1,0:T(8,128)(2,1)} %get-tuple-element.39), channel_id=1, source_target_pairs={{0,4},{1,5},{2,6},{3,7},{4,0},{5,1},{6,2},{7,3},{8,12},{9,13},{10,... | collective-permute-start | bytes 393224 | tf_op jit(solution)/shard_map/ppermute | solution.py:48
  77.8 28.9 %collective-permute-start = (bf16[128,1152]{1,0:T(8,128)(2,1)S(1)}, bf16[128,1152]{1,0:T(8,128)(2,1)}, u32[]{:S(2)}, u32[]{:S(2)}) collective-permute-start(bf16[128,1152]{1,0:T(8,128)(2,1)S(1)} %pad_maximum_fusion.refs_0_), channel_id=1, source_target_pairs={{0,1},{1,0},{2,3},{3,2},{4,5},{5,4},{6,7},{7,6},{8,9},{9,8},{10,11... | collective-permute-start | bytes 884744 | tf_op jit(solution)/shard_map/ppermute | solution.py:48
  80.7 26.0 %collective-permute-start.2 = (bf16[128,1152]{1,0:T(8,128)(2,1)S(1)}, bf16[128,1152]{1,0:T(8,128)(2,1)}, u32[]{:S(2)}, u32[]{:S(2)}) collective-permute-start(bf16[128,1152]{1,0:T(8,128)(2,1)S(1)} %collective-permute-done.1.refs_2_), channel_id=1, source_target_pairs={{0,1},{1,0},{2,3},{3,2},{4,5},{5,4},{6,7},{7,6},{8,9},{9,8},{10,11... | collective-permute-start | bytes 884744 | tf_op jit(solution)/shard_map/ppermute | solution.py:48
  80.7 26.0 %collective-permute-start.4 = (bf16[128,1152]{1,0:T(8,128)(2,1)}, bf16[128,1152]{1,0:T(8,128)(2,1)}, u32[]{:S(2)}, u32[]{:S(2)}) collective-permute-start(bf16[128,1152]{1,0:T(8,128)(2,1)} %collective-permute-done.3.refs_4_), channel_id=1, source_target_pairs={{0,1},{1,0},{2,3},{3,2},{4,5},{5,4},{6,7},{7,6},{8,9},{9,8},{10,11... | collective-permute-start | bytes 884744 | tf_op jit(solution)/shard_map/ppermute | solution.py:48
  81.3 25.5 %collective-permute-start.6 = (bf16[128,1152]{1,0:T(8,128)(2,1)}, bf16[128,1152]{1,0:T(8,128)(2,1)}, u32[]{:S(2)}, u32[]{:S(2)}) collective-permute-start(bf16[128,1152]{1,0:T(8,128)(2,1)} %collective-permute-done.5.refs_6_), channel_id=1, source_target_pairs={{0,1},{1,0},{2,3},{3,2},{4,5},{5,4},{6,7},{7,6},{8,9},{9,8},{10,11... | collective-permute-start | bytes 884744 | tf_op jit(solution)/shard_map/ppermute | solution.py:48
  81.4 20.1 %collective-permute-start.22 = (bf16[32,16,128]{2,1,0:T(8,128)(2,1)}, bf16[32,16,128]{2,1,0:T(8,128)(2,1)}, u32[]{:S(2)}, u32[]{:S(2)}) collective-permute-start(bf16[32,16,128]{2,1,0:T(8,128)(2,1)} %get-tuple-element.40), channel_id=1, source_target_pairs={{0,5},{1,4},{2,7},{3,6},{4,1},{5,0},{6,3},{7,2},{8,13},{9,12},{10,... | collective-permute-start | bytes 393224 | tf_op jit(solution)/shard_map/ppermute | solution.py:48
  (29 other events, 571.4 us)
where the time goes:
time: 124 us; the launch traced here: 122 us
  starting transfers between devices  45 us (36%)
  Pallas kernels  31.9 us (26%)
  waiting for transfers between devices  29.5 us (24%)
  blocking collectives  10.8 us (9%)
  local copies, waits for them, and re-layouts  2.95 us (2%)
    ppermute x28, starting transfers between devices, moved(): return lax.ppermute(part, TP, pairs)  28.3 us
    pallas_call x3, Pallas kernels, shards(): pl.pallas_call(kernel, out_shape=shape((heads, BLOCK, lat_w)) if last els...  18.5 us
    ppermute x28, waiting for transfers between devices, moved(): return lax.ppermute(part, TP, pairs)  14.3 us
    all_to_all x1, starting transfers between devices, shards(): asked = lax.all_to_all(wanted, KV, split_axis=0, concat_axis=0, tiled=True)  11.7 us
    all_to_all x1, blocking collectives, shards(): res = lax.all_to_all(res, TP, split_axis=0, concat_axis=0, tiled=True)  10.8 us
    all_to_all x1, waiting for transfers between devices, shards(): got = lax.all_to_all(send, KV, split_axis=0, concat_axis=0, tiled=True)  7.98 us
    all_to_all x1, waiting for transfers between devices, shards(): asked = lax.all_to_all(wanted, KV, split_axis=0, concat_axis=0, tiled=True)  7.3 us
    all_to_all x1, starting transfers between devices, shards(): got = lax.all_to_all(send, KV, split_axis=0, concat_axis=0, tiled=True)  4.98 us
  transfers between devices with their start and end apart: 30, of which 11 were waited for; matrix products, arithmetic and copies ran while one was open for 0% of the time, Pallas kernels for 24%

commit v1 on v0

v1 whole, which is shorter than its diff:
```python
import math

import jax
import jax.numpy as jnp
from jax import lax
from jax.experimental import pallas as pl
from jax.experimental.pallas import tpu as pltpu
from jax.sharding import Mesh
from jax.sharding import PartitionSpec as P


BLOCK = 128
PER_OWNER = 2
KV = ("kv_0", "kv_1")
TP = ("x", "core")
CHIPS = 4
CORES = 2
ROWS = 512
LANES = 256

STEPS = (0, 1, 3, 2)
SOURCES = [(dx, dc) for dc in (0, 1) for dx in STEPS]


epsilon = 1e-06
f32 = jnp.float32
bf16 = jnp.bfloat16
i32 = jnp.int32

VMEM = pl.BlockSpec(memory_space=pltpu.VMEM)
SMEM = pl.BlockSpec(memory_space=pltpu.SMEM)
ANY = pl.BlockSpec(memory_space=pl.ANY)


def chip_at(step):
    return lax.rem(lax.axis_index("x") + step + CHIPS, CHIPS)


def came_from(source):
    dx, dc = source
    core = lax.axis_index("core")
    return CORES * chip_at(-dx) + (core if dc == 0 else 1 - core)


def over_x(parts):
    out = [parts[0]]
    for part, dx in zip(parts[1:], STEPS[1:]):
        out.append(lax.ppermute(part, "x", [(i, (i + dx) % CHIPS) for i in range(CHIPS)]))
    return out


def with_partner(parts):
    return parts + [lax.ppermute(p, "core", [(0, 1), (1, 0)]) for p in parts]


def normed(values, gain_row):
    wide = values.astype(f32)
    mean_sq = jnp.mean(wide * wide, axis=-1, keepdims=True)
    return (wide * lax.rsqrt(mean_sq + epsilon) * gain_row).astype(bf16)


def side_by_side(ref):
    return jnp.concatenate([ref[i] for i in range(ref.shape[0])], axis=1)


def prepare_kernel(tokens, chosen, qw, ow, up, *outs):
    bufs, (bundle, wanted, table, count) = outs[:-4], outs[-4:]
    blocks = tokens.shape[0] // BLOCK
    sl = BLOCK // (CHIPS * CORES)
    owners = wanted.shape[0]
    for buf, dx in zip(bufs, STEPS):
        for core in range(CORES):
            dest = CORES * chip_at(dx) + core
            buf[core, 0] = tokens[pl.ds(pl.multiple_of(dest * BLOCK, BLOCK), BLOCK), :]
            for b in range(blocks):
                at = pl.multiple_of(b * BLOCK + dest * sl, sl)
                buf[core, 1, b * sl : (b + 1) * sl, :] = tokens[pl.ds(at, sl), :]
    at = qw.shape[0]
    bundle[:at] = qw[...]
    for c in range(0, ow.shape[1], LANES):
        bundle[at : at + ow.shape[0]] = ow[:, c : c + LANES]
        at += ow.shape[0]
    bundle[at:, : up.shape[2]] = up[0]
    bundle[at:, up.shape[2] :] = up[1]
    mine = lax.axis_index(KV[0]) * lax.axis_size(KV[1]) + lax.axis_index(KV[1])
    c = chosen[...]
    valid = c >= 0
    owner = lax.shift_right_arithmetic(c, blocks.bit_length() - 1)
    local = c & (blocks - 1)
    lowest = jnp.zeros_like(c)
    lane = lax.broadcasted_iota(i32, (1, wanted.shape[2]), 1)
    for o in range(owners):
        hit = owner == o
        low = jnp.min(jnp.where(hit, local, blocks - 1), keepdims=True)
        high = jnp.max(jnp.where(hit, local, 0), keepdims=True)
        wanted[o] = jnp.where(lane == 0, low, high)
        lowest = jnp.where(hit, low, lowest)
    far = blocks + owner * PER_OWNER + jnp.where(local == lowest, 0, 1)
    table[...] = jnp.where(valid, jnp.where(owner == mine, local, far), 0)
    count[...] = jnp.broadcast_to(
        jnp.sum(jnp.where(valid, 1.0, 0.0), axis=1, keepdims=True).astype(i32), count.shape
    )


def latent_kernel(asked, lw, *refs):
    toks, (lat_out, send_out, tok) = refs[:-3], refs[-3:]
    for part, source in zip(toks, SOURCES):
        tok[came_from(source)] = part[lax.axis_index("core"), 1]
    lat = jnp.dot(side_by_side(tok), lw[...], preferred_element_type=f32).astype(bf16)
    lat_out[...] = lat.reshape(lat_out.shape)
    for o in range(send_out.shape[0]):
        for s in range(PER_OWNER):
            send_out[o, s] = lat_out[asked[o, 0, s]]


def pick_kernel(table, own, got, *refs):
    outs, pool = refs[:-1], refs[-1]
    blocks = own.shape[0]
    pool[:blocks] = own[...]
    pool[blocks:] = got[...]
    for out, dx in zip(outs, STEPS):
        for core in range(CORES):
            dest = CORES * chip_at(dx) + core
            for c in range(out.shape[1]):
                out[core, c] = pool[table[dest, c]]


def query_kernel(gain, *refs):
    n = len(SOURCES)
    toks, pieces, (out, tok, weights, sem) = refs[:n], refs[n : 2 * n], refs[2 * n :]
    fetch = [
        pltpu.make_async_copy(p.at[pl.ds(0, weights.shape[1])], weights.at[i], sem.at[i])
        for i, p in enumerate(pieces)
    ]
    for copy in fetch:
        copy.start()
    for part, source in zip(toks, SOURCES):
        tok[came_from(source)] = part[lax.axis_index("core"), 0]
    lhs = side_by_side(tok)
    width = gain.shape[1]
    heads = out.shape[0] // n
    for i in range(n):
        fetch[i].wait()
        acc = jnp.dot(lhs, weights[i], preferred_element_type=f32).astype(bf16)
        for h in range(heads):
            out[i * heads + h] = normed(acc[:, h * width : (h + 1) * width], gain[...])


def attend_kernel(count, q_ref, kgain, ogain, *refs):
    n = len(SOURCES)
    pieces, bundles, (out, kv, weights, acc, kv_sem, weight_sem) = refs[:n], refs[n : 2 * n], refs[2 * n :]
    mine = lax.axis_index("core")
    fetch = [pltpu.make_async_copy(p.at[mine], kv.at[i], kv_sem.at[i]) for i, p in enumerate(pieces)]
    first = bundles[0].shape[0] - weights.shape[1]
    later = [
        pltpu.make_async_copy(b.at[pl.ds(first, weights.shape[1])], weights.at[i], weight_sem.at[i])
        for i, b in enumerate(bundles)
    ]
    for copy in fetch + later:
        copy.start()
    _, picks, sl, width = kv.shape
    keys = picks * sl
    heads = q_ref.shape[0]
    per = ROWS // BLOCK
    here = count[came_from((0, 0)), 0]
    gain = kgain[...] * (width**-0.5 * math.log2(math.e))
    on = lax.broadcasted_iota(i32, (keys, width), 0) < here * sl
    at = lax.broadcasted_iota(i32, (ROWS, BLOCK), 1)
    row = lax.broadcasted_iota(i32, (ROWS, BLOCK), 0) & (BLOCK - 1)
    for i, source in enumerate(SOURCES):
        fetch[i].wait()
        src = came_from(source)
        lat = kv[i].reshape(keys, width)
        lat = jnp.where(on, lat, jnp.zeros_like(lat))
        ones = jnp.where(on, jnp.ones_like(lat), jnp.zeros_like(lat))
        k = normed(lat, gain)
        v = jnp.concatenate([lat, ones], axis=1)
        for r in range(heads // per):
            q = jnp.concatenate([q_ref[r * per + h] for h in range(per)], axis=0)
            s = lax.dot_general(q, k, (((1,), (1,)), ((), ())), preferred_element_type=f32)
            w = jnp.exp2(s)
            own = jnp.where((at >= sl) | (at + src * sl <= row), w[:, :BLOCK], 0.0)
            w = jnp.concatenate([own, w[:, BLOCK:]], axis=1).astype(bf16)
            got = jnp.dot(w, v, preferred_element_type=f32)
            acc[r] = got if i == 0 else acc[r] + got
    for copy in later:
        copy.wait()
    model = ogain.shape[1]
    total = None
    for i in range(n):
        block = weights[i]
        rows = model // LANES * BLOCK
        up = jnp.concatenate([block[rows:, :width], block[rows:, width:]], axis=0)
        halves = []
        for h in (CORES * i, CORES * i + 1):
            r, k = h // per, h % per
            sums = acc[r, k * BLOCK : (k + 1) * BLOCK, :]
            att = (sums[:, :width] / sums[:, width:]).astype(bf16)
            halves.append(
                lax.dot_general(att, up, (((1,), (1,)), ((), ())), preferred_element_type=f32)
            )
        lane = lax.broadcasted_iota(i32, halves[0].shape, 1)
        side = jnp.where(lane < width // CORES, halves[0], halves[1]).astype(bf16)
        proj = jnp.concatenate(
            [block[c * BLOCK : (c + 1) * BLOCK] for c in range(model // LANES)], axis=1
        )
        part = jnp.dot(side, proj, preferred_element_type=f32)
        total = part if total is None else total + part
    mean_sq = jnp.mean(total * total, axis=-1, keepdims=True)
    res = (total * lax.rsqrt(mean_sq + epsilon) * ogain[...]).astype(bf16)
    w = out.shape[2]
    for p in range(out.shape[0]):
        out[p] = res[:, p * w : (p + 1) * w]


def shape(dims, kind=bf16):
    return jax.ShapeDtypeStruct(dims, kind)


def shards(
    tokens,
    query_weight,
    latent_weight,
    query_gain,
    key_gain,
    value_up,
    out_weight,
    out_gain,
    chosen,
):
    rows, feats = tokens.shape
    lat_w = latent_weight.shape[1]
    blocks = rows // BLOCK
    picks = chosen.shape[1]
    owners = lax.axis_size(KV)
    tp = len(SOURCES)
    sl = BLOCK // tp
    heads = query_weight.shape[1] // lat_w * tp
    q_rows = query_weight.shape[0]
    late_rows = (out_weight.size + value_up.size) // LANES

    *bufs, bundle, wanted, table, count = pl.pallas_call(
        prepare_kernel,
        out_shape=[shape((CORES, 2, BLOCK, feats))] * CHIPS
        + [
            shape((q_rows + late_rows, LANES)),
            shape((owners, 1, BLOCK), i32),
            shape((blocks, picks), i32),
            shape((blocks, BLOCK), i32),
        ],
        in_specs=[VMEM] * 5,
        out_specs=[VMEM] * (CHIPS + 4),
        name="prepare",
    )(tokens, chosen, query_weight, out_weight, value_up.swapaxes(1, 2))

    toks_x = over_x(bufs)
    bundles_x = over_x([bundle] * CHIPS)
    asked = lax.all_to_all(wanted, KV, split_axis=0, concat_axis=0, tiled=True)
    toks = with_partner(toks_x)

    latent, send = pl.pallas_call(
        latent_kernel,
        out_shape=(shape((blocks, sl, lat_w)), shape((owners, PER_OWNER, sl, lat_w))),
        in_specs=[SMEM] + [VMEM] * (tp + 1),
        out_specs=(VMEM, VMEM),
        scratch_shapes=[pltpu.VMEM((tp, BLOCK, feats), bf16)],
        name="latent",
    )(asked, latent_weight, *toks)

    got = lax.all_to_all(send, KV, split_axis=0, concat_axis=0, tiled=True)
    got = got.reshape(owners * PER_OWNER, sl, lat_w)

    picked = pl.pallas_call(
        pick_kernel,
        out_shape=[shape((CORES, picks, sl, lat_w))] * CHIPS,
        in_specs=[SMEM, VMEM, VMEM],
        out_specs=[VMEM] * CHIPS,
        scratch_shapes=[pltpu.VMEM((blocks + owners * PER_OWNER, sl, lat_w), bf16)],
        name="pick",
    )(table, latent, got)
    kv = with_partner(over_x(picked))
    bundles = with_partner(bundles_x)

    q = pl.pallas_call(
        query_kernel,
        out_shape=shape((heads, BLOCK, lat_w)),
        in_specs=[VMEM] * (tp + 1) + [ANY] * tp,
        out_specs=VMEM,
        scratch_shapes=[
            pltpu.VMEM((tp, BLOCK, feats), bf16),
            pltpu.VMEM((tp, q_rows, LANES), bf16),
            pltpu.SemaphoreType.DMA((tp,)),
        ],
        name="query",
    )(query_gain[None, :], *toks, *bundles)

    width = out_weight.shape[1] // tp
    res = pl.pallas_call(
        attend_kernel,
        out_shape=shape((tp, BLOCK, width)),
        in_specs=[SMEM] + [VMEM] * 3 + [ANY] * (2 * tp),
        out_specs=VMEM,
        scratch_shapes=[
            pltpu.VMEM((tp, picks, sl, lat_w), bf16),
            pltpu.VMEM((tp, late_rows, LANES), bf16),
            pltpu.VMEM((heads * BLOCK // ROWS, ROWS, 2 * lat_w), f32),
            pltpu.SemaphoreType.DMA((tp,)),
            pltpu.SemaphoreType.DMA((tp,)),
        ],
        name="attend",
    )(count, q, key_gain[None, :], out_gain[None, :], *kv, *bundles)

    res = lax.all_to_all(res, TP, split_axis=0, concat_axis=0, tiled=True)
    return res.reshape(rows, width)


def solution(mesh):
    torus = Mesh(mesh.devices.reshape(8, 4, CHIPS, CORES), ("kv_0", "kv_1", "x", "core"))
    in_specs = (
        P(KV, TP),
        P(None, TP),
        P(),
        P(),
        P(),
        P(TP, None, None),
        P(TP, None),
        P(),
        P(KV, None),
    )
    return jax.shard_map(
        shards, mesh=torus, in_specs=in_specs, out_specs=P(KV, TP), check_vma=False
    )
```

time: 124 us -> 145 us (1.17)
  the two profiles are of different devices: /device:TPU:8 before, /device:TPU:1 now
where the time goes in v1:
time: 145 us
  blocking collectives  46.8 us (32%)
  starting transfers between devices  37.3 us (26%)
  waiting for transfers between devices  29.6 us (20%)
  Pallas kernels  29.5 us (20%)
  local copies, waits for them, and re-layouts  1.49 us (1%)
    all_to_all x1, blocking collectives, shards(): asked = lax.all_to_all(wanted, KV, split_axis=0, concat_axis=0, tiled=True)  35.9 us
    ppermute x9, waiting for transfers between devices, over_x(): lax.ppermute(part, 'x', [(i, (i + dx) % CHIPS) for i in range(CHIPS)])  20.6 us
    ppermute x12, starting transfers between devices, with_partner(): return parts + [lax.ppermute(p, 'core', [(0, 1), (1, 0)]) for p in parts]  18.9 us
    pallas_call x1, Pallas kernels, shards(): pl.pallas_call(attend_kernel, out_shape=shape((tp, BLOCK, width)), in_spe...  16.1 us
    ppermute x9, starting transfers between devices, over_x(): lax.ppermute(part, 'x', [(i, (i + dx) % CHIPS) for i in range(CHIPS)])  14.6 us
    all_to_all x1, blocking collectives, shards(): res = lax.all_to_all(res, TP, split_axis=0, concat_axis=0, tiled=True)  10.9 us
    all_to_all x1, waiting for transfers between devices, shards(): got = lax.all_to_all(send, KV, split_axis=0, concat_axis=0, tiled=True)  8.12 us
    pallas_call x1, Pallas kernels, shards(): pl.pallas_call(query_kernel, out_shape=shape((heads, BLOCK, lat_w)), in_s...  6.24 us
  transfers between devices with their start and end apart: 22, of which 5 were waited for; matrix products, arithmetic and copies ran while one was open for 0% of the time, Pallas kernels for 7%

profile of v1, /device:TPU:1, one launch (start us, length us, event | category | flops | bytes accessed | tf_op | source)
XLA Modules:
  0.0 144.9 jit_solution(8184468828671333744)
XLA Ops:
  0.0 2.6 %prepare.1 = (bf16[2,2,128,128]{3,2,1,0:T(8,128)(2,1)}, bf16[2,2,128,128]{3,2,1,0:T(8,128)(2,1)}, bf16[2,2,128,128]{3,2,1,0:T(8,128)(2,1)}, bf16[2,2,128,128]{3,...) custom-call(bf16[1024,128]{1,0:T(8,128)(2,1)} %tokens.1, ...), custom_call_target="tpu_custom_call" | custom-call | tf_op jit(solution)/shard_map/prepare/pallas_call | solution.py:242
  2.6 2.0 %collective-permute-start.7 = (bf16[1600,256]{1,0:T(8,128)(2,1)}, bf16[1600,256]{1,0:T(8,128)(2,1)S(1)}, u32[]{:S(2)}, u32[]{:S(2)}) collective-permute-start(bf16[1600,256]{1,0:T(8,128)(2,1)} %get-tuple-element.24.refs_8_), channel_id=1, source_target_pairs={{0,2},{2,4},{4,6},{6,0},{1,3},{3,5},{5,7},{7,1},{8,10},{10,12},{12... | collective-permute-start | bytes 2457608 | tf_op jit(solution)/shard_map/ppermute | solution.py:48
  4.6 1.3 collective-permute-start.8
  6.1 2.6 %collective-permute-start.1 = (bf16[2,2,128,128]{3,2,1,0:T(8,128)(2,1)}, bf16[2,2,128,128]{3,2,1,0:T(8,128)(2,1)S(1)}, u32[]{:S(2)}, u32[]{:S(2)}) collective-permute-start(bf16[2,2,128,128]{3,2,1,0:T(8,128)(2,1)} %get-tuple-element.22), channel_id=1, source_target_pairs={{0,6},{2,0},{4,2},{6,4},{1,7},{3,1},{5,3},{7,5},{8,14},{10,8},{12,... | collective-permute-start | bytes 393224 | tf_op jit(solution)/shard_map/ppermute | solution.py:48
  9.1 15.6 %collective-permute-done.refs_1_ = bf16[2,2,128,128]{3,2,1,0:T(8,128)(2,1)S(1)} collective-permute-done((bf16[2,2,128,128]{3,2,1,0:T(8,128)(2,1)}, bf16[2,2,128,128]{3,2,1,0:T(8,128)(2,1)S(1)}, u32[]{:S(2)}, u32[]{:S(2)}) %collective-permute-start) | collective-permute-done | bytes 131104 | tf_op jit(solution)/shard_map/ppermute | solution.py:48
  24.7 3.9 %collective-permute-start.9 = (bf16[1600,256]{1,0:T(8,128)(2,1)}, bf16[1600,256]{1,0:T(8,128)(2,1)S(1)}, u32[]{:S(2)}, u32[]{:S(2)}) collective-permute-start(bf16[1600,256]{1,0:T(8,128)(2,1)} %get-tuple-element.24.refs_8_), channel_id=1, source_target_pairs={{0,4},{2,6},{4,0},{6,2},{1,5},{3,7},{5,1},{7,3},{8,12},{10,14},{12... | collective-permute-start | bytes 2457608 | tf_op jit(solution)/shard_map/ppermute | solution.py:48
  28.5 2.9 %collective-permute-start.3 = (bf16[2,2,128,128]{3,2,1,0:T(8,128)(2,1)}, bf16[2,2,128,128]{3,2,1,0:T(8,128)(2,1)S(1)}, u32[]{:S(2)}, u32[]{:S(2)}) collective-permute-start(bf16[2,2,128,128]{3,2,1,0:T(8,128)(2,1)} %get-tuple-element.20.refs_0_), channel_id=1, source_target_pairs={{0,1},{1,0},{2,3},{3,2},{4,5},{5,4},{6,7},{7,6},{8,9},{9,8},{10,11... | collective-permute-start | bytes 393224 | tf_op jit(solution)/shard_map/ppermute | solution.py:53
  31.5 1.7 %collective-permute-start.4 = (bf16[2,2,128,128]{3,2,1,0:T(8,128)(2,1)S(1)}, bf16[2,2,128,128]{3,2,1,0:T(8,128)(2,1)S(1)}, u32[]{:S(2)}, u32[]{:S(2)}) collective-permute-start(bf16[2,2,128,128]{3,2,1,0:T(8,128)(2,1)S(1)} %collective-permute-done.refs_1_), channel_id=1, source_target_pairs={{0,1},{1,0},{2,3},{3,2},{4,5},{5,4},{6,7},{7,6},{8,9},{9,8},{10,11... | collective-permute-start | bytes 393224 | tf_op jit(solution)/shard_map/ppermute | solution.py:53
  33.3 0.9 collective-permute-done.4.refs_5_
  34.8 35.9 %all_to_all.15.asked = s32[32,1,128]{2,1,0:T(1,128)} all-to-all(s32[32,1,128]{2,1,0:T(1,128)} %get-tuple-element.26), channel_id=1, replica_groups=mesh['kv_0'=8,'kv_1'=4,'x'=4,'core'=2] {'kv_0','kv_1'}, dimensions={0} | all-to-all | bytes 32768 | tf_op jit(solution)/shard_map/all_to_all | solution.py:258
  70.7 2.4 %latent.1 = (bf16[8,16,128]{2,1,0:T(8,128)(2,1)}, bf16[32,2,16,128]{3,2,1,0:T(8,128)(2,1)}) custom-call(s32[32,1,128]{2,1,0:T(1,128)} %all_to_all.15.asked, bf16[1024,128]{1,0:T(8,128)(2,1)} %lw.1, bf16[2,2,128,128]{3,2,1,0:T(8,128)(2,1)} %get-tuple-element.20.refs_0_, bf16[2,2,128,128]{3,2,1,0:T(8,128)(2,1)} %copy-done.5, ...), custom_call_target="tpu_custom_call" | custom-call | tf_op jit(solution)/shard_map/latent/pallas_call | solution.py:261
  73.1 3.9 %all-to-all-start.1 = ((bf16[32,2,16,128]{3,2,1,0:T(8,128)(2,1)}), bf16[32,2,16,128]{3,2,1,0:T(8,128)(2,1)S(1)}, u32[]{:S(2)}, u32[]{:S(2)}) async-start(bf16[32,2,16,128]{3,2,1,0:T(8,128)(2,1)} %get-tuple-element.28), calls=%async_computation.1 | async-start | bytes 524288 | tf_op jit(solution)/shard_map/all_to_all | solution.py:270
  77.0 1.9 %collective-permute-start.11 = (bf16[1600,256]{1,0:T(8,128)(2,1)S(1)}, bf16[1600,256]{1,0:T(8,128)(2,1)}, u32[]{:S(2)}, u32[]{:S(2)}) collective-permute-start(bf16[1600,256]{1,0:T(8,128)(2,1)S(1)} %collective-permute-done.7.refs_9_), channel_id=1, source_target_pairs={{0,1},{1,0},{2,3},{3,2},{4,5},{5,4},{6,7},{7,6},{8,9},{9,8},{10,11... | collective-permute-start | bytes 2457608 | tf_op jit(solution)/shard_map/ppermute | solution.py:53
  79.4 8.1 %all-to-all-done.1 = bf16[32,2,16,128]{3,2,1,0:T(8,128)(2,1)S(1)} async-done(((bf16[32,2,16,128]{3,2,1,0:T(8,128)(2,1)}), bf16[32,2,16,128]{3,2,1,0:T(8,128)(2,1)S(1)}, u32[]{:S(2)}, u32[]{:S(2)}) %all-to-all-start.1) | async-done | bytes 262176 | tf_op jit(solution)/shard_map/all_to_all | solution.py:270
  88.2 2.1 %pick.1 = (bf16[2,32,16,128]{3,2,1,0:T(8,128)(2,1)}, bf16[2,32,16,128]{3,2,1,0:T(8,128)(2,1)}, bf16[2,32,16,128]{3,2,1,0:T(8,128)(2,1)}, bf16[2,32,16,128]{3,2,1,0:T(8,128)(2,1)}) custom-call(s32[8,32]{1,0:T(8,128)} %get-tuple-element.25.table, bf16[8,16,128]{2,1,0:T(8,128)(2,1)} %get-tuple-element.27.own, bf16[64,16,128]{2,1,0:T(8,128)(2,1)} %bitcast.6), custom_call_target="tpu_custom_call" | custom-call | tf_op jit(solution)/shard_map/pick/pallas_call | solution.py:273
  90.4 3.4 %collective-permute-start.15 = (bf16[2,32,16,128]{3,2,1,0:T(8,128)(2,1)}, bf16[2,32,16,128]{3,2,1,0:T(8,128)(2,1)}, u32[]{:S(2)}, u32[]{:S(2)}) collective-permute-start(bf16[2,32,16,128]{3,2,1,0:T(8,128)(2,1)} %get-tuple-element.31), channel_id=1, source_target_pairs={{0,6},{2,0},{4,2},{6,4},{1,7},{3,1},{5,3},{7,5},{8,14},{10,8},{12,... | collective-permute-start | bytes 786440 | tf_op jit(solution)/shard_map/ppermute | solution.py:48
  93.7 3.9 %collective-permute-done.14.refs_1_ = bf16[2,32,16,128]{3,2,1,0:T(8,128)(2,1)S(1)} collective-permute-done((bf16[2,32,16,128]{3,2,1,0:T(8,128)(2,1)}, bf16[2,32,16,128]{3,2,1,0:T(8,128)(2,1)S(1)}, u32[]{:S(2)}, u32[]{:S(2)}) %collective-permute-start.14) | collective-permute-done | bytes 262176 | tf_op jit(solution)/shard_map/ppermute | solution.py:48
  97.6 0.8 collective-permute-start.16
  98.5 6.2 %collective-permute-start.17 = (bf16[2,32,16,128]{3,2,1,0:T(8,128)(2,1)}, bf16[2,32,16,128]{3,2,1,0:T(8,128)(2,1)}, u32[]{:S(2)}, u32[]{:S(2)}) collective-permute-start(bf16[2,32,16,128]{3,2,1,0:T(8,128)(2,1)} %get-tuple-element.29.refs_0_), channel_id=1, source_target_pairs={{0,1},{1,0},{2,3},{3,2},{4,5},{5,4},{6,7},{7,6},{8,9},{9,8},{10,11... | collective-permute-start | bytes 786440 | tf_op jit(solution)/shard_map/ppermute | solution.py:53
  104.6 1.1 collective-permute-done.16.refs_3_
  105.7 4.5 %collective-permute-start.18 = (bf16[2,32,16,128]{3,2,1,0:T(8,128)(2,1)S(1)}, bf16[2,32,16,128]{3,2,1,0:T(8,128)(2,1)}, u32[]{:S(2)}, u32[]{:S(2)}) collective-permute-start(bf16[2,32,16,128]{3,2,1,0:T(8,128)(2,1)S(1)} %collective-permute-done.14.refs_1_), channel_id=1, source_target_pairs={{0,1},{1,0},{2,3},{3,2},{4,5},{5,4},{6,7},{7,6},{8,9},{9,8},{10,11... | collective-permute-start | bytes 786440 | tf_op jit(solution)/shard_map/ppermute | solution.py:53
  110.8 6.2 %query.1.q_ref = bf16[16,128,128]{2,1,0:T(8,128)(2,1)} custom-call(f32[1,128]{1,0:T(1,128)} %bitcast.10, bf16[2,2,128,128]{3,2,1,0:T(8,128)(2,1)} %get-tuple-element.20.refs_0_, bf16[2,2,128,128]{3,2,1,0:T(8,128)(2,1)} %copy-done.5, bf16[2,2,128,128]{3,2,1,0:T(8,128)(2,1)} %copy-done.6, bf16[2,2,128,128]{3,2,1,0:T(8,128)(2,1)} %copy-done.7, ...), custom_call_target="tpu_custom_call" | custom-call | tf_op jit(solution)/shard_map/query/pallas_call | solution.py:284
  117.1 16.1 %attend.1 = bf16[8,128,128]{2,1,0:T(8,128)(2,1)} custom-call(s32[8,128]{1,0:T(8,128)} %get-tuple-element.19.count, bf16[16,128,128]{2,1,0:T(8,128)(2,1)} %query.1.q_ref, f32[1,128]{1,0:T(1,128)} %bitcast.11, f32[1,1024]{1,0:T(1,128)} %bitcast.9, bf16[2,32,16,128]{3,2,1,0:T(8,128)(2,1)} %get-tuple-element.29.refs_0_, bf16[2,32,16,128]{3,2,1,0:T(8,128)(2,1)} %copy-done.11, ...), custom_call_target="tpu_custom_call" | custom-call | tf_op jit(solution)/shard_map/attend/pallas_call | solution.py:298
  133.2 10.9 %all_to_all.16 = bf16[8,128,128]{2,1,0:T(8,128)(2,1)S(1)} all-to-all(bf16[8,128,128]{2,1,0:T(8,128)(2,1)} %attend.1), channel_id=1, replica_groups=mesh['kv_0'=8,'kv_1'=4,'x'=4,'core'=2] {'x','core'}, dimensions={0} | all-to-all | bytes 524288 | tf_op jit(solution)/shard_map/all_to_all | solution.py:313
  (52 shorter events, 3.8 us)
Async XLA Ops:
  2.6 74.4 %collective-permute-start.7 = (bf16[1600,256]{1,0:T(8,128)(2,1)}, bf16[1600,256]{1,0:T(8,128)(2,1)S(1)}, u32[]{:S(2)}, u32[]{:S(2)}) collective-permute-start(bf16[1600,256]{1,0:T(8,128)(2,1)} %get-tuple-element.24.refs_8_), channel_id=1, source_target_pairs={{0,2},{2,4},{4,6},{6,0},{1,3},{3,5},{5,7},{7,1},{8,10},{10,12},{12... | collective-permute-start | bytes 2457608 | tf_op jit(solution)/shard_map/ppermute | solution.py:48
  4.6 74.3 %collective-permute-start.8 = (bf16[1600,256]{1,0:T(8,128)(2,1)}, bf16[1600,256]{1,0:T(8,128)(2,1)S(1)}, u32[]{:S(2)}, u32[]{:S(2)}) collective-permute-start(bf16[1600,256]{1,0:T(8,128)(2,1)} %get-tuple-element.24.refs_8_), channel_id=1, source_target_pairs={{0,6},{2,0},{4,2},{6,4},{1,7},{3,1},{5,3},{7,5},{8,14},{10,8},{12,... | collective-permute-start | bytes 2457608 | tf_op jit(solution)/shard_map/ppermute | solution.py:48
  6.0 18.7 %collective-permute-start = (bf16[2,2,128,128]{3,2,1,0:T(8,128)(2,1)}, bf16[2,2,128,128]{3,2,1,0:T(8,128)(2,1)S(1)}, u32[]{:S(2)}, u32[]{:S(2)}) collective-permute-start(bf16[2,2,128,128]{3,2,1,0:T(8,128)(2,1)} %get-tuple-element.21), channel_id=1, source_target_pairs={{0,2},{2,4},{4,6},{6,0},{1,3},{3,5},{5,7},{7,1},{8,10},{10,12},{12... | collective-permute-start | bytes 393224 | tf_op jit(solution)/shard_map/ppermute | solution.py:48
  6.1 22.5 %collective-permute-start.1 = (bf16[2,2,128,128]{3,2,1,0:T(8,128)(2,1)}, bf16[2,2,128,128]{3,2,1,0:T(8,128)(2,1)S(1)}, u32[]{:S(2)}, u32[]{:S(2)}) collective-permute-start(bf16[2,2,128,128]{3,2,1,0:T(8,128)(2,1)} %get-tuple-element.22), channel_id=1, source_target_pairs={{0,6},{2,0},{4,2},{6,4},{1,7},{3,1},{5,3},{7,5},{8,14},{10,8},{12,... | collective-permute-start | bytes 393224 | tf_op jit(solution)/shard_map/ppermute | solution.py:48
  8.6 22.8 %collective-permute-start.2 = (bf16[2,2,128,128]{3,2,1,0:T(8,128)(2,1)}, bf16[2,2,128,128]{3,2,1,0:T(8,128)(2,1)S(1)}, u32[]{:S(2)}, u32[]{:S(2)}) collective-permute-start(bf16[2,2,128,128]{3,2,1,0:T(8,128)(2,1)} %get-tuple-element.23), channel_id=1, source_target_pairs={{0,4},{2,6},{4,0},{6,2},{1,5},{3,7},{5,1},{7,3},{8,12},{10,14},{12... | collective-permute-start | bytes 393224 | tf_op jit(solution)/shard_map/ppermute | solution.py:48
  24.7 46.1 %copy-start.5 = (bf16[2,2,128,128]{3,2,1,0:T(8,128)(2,1)}, bf16[2,2,128,128]{3,2,1,0:T(8,128)(2,1)S(1)}, u32[]{:S(2)}) copy-start(bf16[2,2,128,128]{3,2,1,0:T(8,128)(2,1)S(1)} %collective-permute-done.refs_1_) | copy-start | bytes 393220
  24.7 54.3 %collective-permute-start.9 = (bf16[1600,256]{1,0:T(8,128)(2,1)}, bf16[1600,256]{1,0:T(8,128)(2,1)S(1)}, u32[]{:S(2)}, u32[]{:S(2)}) collective-permute-start(bf16[1600,256]{1,0:T(8,128)(2,1)} %get-tuple-element.24.refs_8_), channel_id=1, source_target_pairs={{0,4},{2,6},{4,0},{6,2},{1,5},{3,7},{5,1},{7,3},{8,12},{10,14},{12... | collective-permute-start | bytes 2457608 | tf_op jit(solution)/shard_map/ppermute | solution.py:48
  28.5 42.2 %copy-start.6 = (bf16[2,2,128,128]{3,2,1,0:T(8,128)(2,1)}, bf16[2,2,128,128]{3,2,1,0:T(8,128)(2,1)S(1)}, u32[]{:S(2)}) copy-start(bf16[2,2,128,128]{3,2,1,0:T(8,128)(2,1)S(1)} %collective-permute-done.1.refs_2_) | copy-start | bytes 393220
  28.5 4.7 %collective-permute-start.3 = (bf16[2,2,128,128]{3,2,1,0:T(8,128)(2,1)}, bf16[2,2,128,128]{3,2,1,0:T(8,128)(2,1)S(1)}, u32[]{:S(2)}, u32[]{:S(2)}) collective-permute-start(bf16[2,2,128,128]{3,2,1,0:T(8,128)(2,1)} %get-tuple-element.20.refs_0_), channel_id=1, source_target_pairs={{0,1},{1,0},{2,3},{3,2},{4,5},{5,4},{6,7},{7,6},{8,9},{9,8},{10,11... | collective-permute-start | bytes 393224 | tf_op jit(solution)/shard_map/ppermute | solution.py:53
  31.5 2.7 %collective-permute-start.4 = (bf16[2,2,128,128]{3,2,1,0:T(8,128)(2,1)S(1)}, bf16[2,2,128,128]{3,2,1,0:T(8,128)(2,1)S(1)}, u32[]{:S(2)}, u32[]{:S(2)}) collective-permute-start(bf16[2,2,128,128]{3,2,1,0:T(8,128)(2,1)S(1)} %collective-permute-done.refs_1_), channel_id=1, source_target_pairs={{0,1},{1,0},{2,3},{3,2},{4,5},{5,4},{6,7},{7,6},{8,9},{9,8},{10,11... | collective-permute-start | bytes 393224 | tf_op jit(solution)/shard_map/ppermute | solution.py:53
  33.2 1.3 collective-permute-start.5
  34.2 36.5 %collective-permute-start.6 = (bf16[2,2,128,128]{3,2,1,0:T(8,128)(2,1)S(1)}, bf16[2,2,128,128]{3,2,1,0:T(8,128)(2,1)}, u32[]{:S(2)}, u32[]{:S(2)}) collective-permute-start(bf16[2,2,128,128]{3,2,1,0:T(8,128)(2,1)S(1)} %collective-permute-done.2.refs_3_), channel_id=1, source_target_pairs={{0,1},{1,0},{2,3},{3,2},{4,5},{5,4},{6,7},{7,6},{8,9},{9,8},{10,11... | collective-permute-start | bytes 393224 | tf_op jit(solution)/shard_map/ppermute | solution.py:53
  34.6 55.8 %collective-permute-start.10 = (bf16[1600,256]{1,0:T(8,128)(2,1)}, bf16[1600,256]{1,0:T(8,128)(2,1)S(1)}, u32[]{:S(2)}, u32[]{:S(2)}) collective-permute-start(bf16[1600,256]{1,0:T(8,128)(2,1)} %get-tuple-element.24.refs_8_), channel_id=1, source_target_pairs={{0,1},{1,0},{2,3},{3,2},{4,5},{5,4},{6,7},{7,6},{8,9},{9,8},{10,11... | collective-permute-start | bytes 2457608 | tf_op jit(solution)/shard_map/ppermute | solution.py:53
  73.1 14.4 %all-to-all-start.1 = ((bf16[32,2,16,128]{3,2,1,0:T(8,128)(2,1)}), bf16[32,2,16,128]{3,2,1,0:T(8,128)(2,1)S(1)}, u32[]{:S(2)}, u32[]{:S(2)}) async-start(bf16[32,2,16,128]{3,2,1,0:T(8,128)(2,1)} %get-tuple-element.28), calls=%async_computation.1 | async-start | bytes 524288 | tf_op jit(solution)/shard_map/all_to_all | solution.py:270
  77.0 33.2 %collective-permute-start.11 = (bf16[1600,256]{1,0:T(8,128)(2,1)S(1)}, bf16[1600,256]{1,0:T(8,128)(2,1)}, u32[]{:S(2)}, u32[]{:S(2)}) collective-permute-start(bf16[1600,256]{1,0:T(8,128)(2,1)S(1)} %collective-permute-done.7.refs_9_), channel_id=1, source_target_pairs={{0,1},{1,0},{2,3},{3,2},{4,5},{5,4},{6,7},{7,6},{8,9},{9,8},{10,11... | collective-permute-start | bytes 2457608 | tf_op jit(solution)/shard_map/ppermute | solution.py:53
  78.9 31.4 %collective-permute-start.12 = (bf16[1600,256]{1,0:T(8,128)(2,1)S(1)}, bf16[1600,256]{1,0:T(8,128)(2,1)}, u32[]{:S(2)}, u32[]{:S(2)}) collective-permute-start(bf16[1600,256]{1,0:T(8,128)(2,1)S(1)} %collective-permute-done.8.refs_10_), channel_id=1, source_target_pairs={{0,1},{1,0},{2,3},{3,2},{4,5},{5,4},{6,7},{7,6},{8,9},{9,8},{10,11... | collective-permute-start | bytes 2457608 | tf_op jit(solution)/shard_map/ppermute | solution.py:53
  79.0 31.7 %collective-permute-start.13 = (bf16[1600,256]{1,0:T(8,128)(2,1)S(1)}, bf16[1600,256]{1,0:T(8,128)(2,1)}, u32[]{:S(2)}, u32[]{:S(2)}) collective-permute-start(bf16[1600,256]{1,0:T(8,128)(2,1)S(1)} %collective-permute-done.9.refs_11_), channel_id=1, source_target_pairs={{0,1},{1,0},{2,3},{3,2},{4,5},{5,4},{6,7},{7,6},{8,9},{9,8},{10,11... | collective-permute-start | bytes 2457608 | tf_op jit(solution)/shard_map/ppermute | solution.py:53
  90.4 7.2 %collective-permute-start.14 = (bf16[2,32,16,128]{3,2,1,0:T(8,128)(2,1)}, bf16[2,32,16,128]{3,2,1,0:T(8,128)(2,1)S(1)}, u32[]{:S(2)}, u32[]{:S(2)}) collective-permute-start(bf16[2,32,16,128]{3,2,1,0:T(8,128)(2,1)} %get-tuple-element.30), channel_id=1, source_target_pairs={{0,2},{2,4},{4,6},{6,0},{1,3},{3,5},{5,7},{7,1},{8,10},{10,12},{12... | collective-permute-start | bytes 786440 | tf_op jit(solution)/shard_map/ppermute | solution.py:48
  90.4 8.1 %collective-permute-start.15 = (bf16[2,32,16,128]{3,2,1,0:T(8,128)(2,1)}, bf16[2,32,16,128]{3,2,1,0:T(8,128)(2,1)}, u32[]{:S(2)}, u32[]{:S(2)}) collective-permute-start(bf16[2,32,16,128]{3,2,1,0:T(8,128)(2,1)} %get-tuple-element.31), channel_id=1, source_target_pairs={{0,6},{2,0},{4,2},{6,4},{1,7},{3,1},{5,3},{7,5},{8,14},{10,8},{12,... | collective-permute-start | bytes 786440 | tf_op jit(solution)/shard_map/ppermute | solution.py:48
  97.6 8.1 %collective-permute-start.16 = (bf16[2,32,16,128]{3,2,1,0:T(8,128)(2,1)}, bf16[2,32,16,128]{3,2,1,0:T(8,128)(2,1)}, u32[]{:S(2)}, u32[]{:S(2)}) collective-permute-start(bf16[2,32,16,128]{3,2,1,0:T(8,128)(2,1)} %get-tuple-element.32), channel_id=1, source_target_pairs={{0,4},{2,6},{4,0},{6,2},{1,5},{3,7},{5,1},{7,3},{8,12},{10,14},{12... | collective-permute-start | bytes 786440 | tf_op jit(solution)/shard_map/ppermute | solution.py:48
  98.5 18.6 %collective-permute-start.17 = (bf16[2,32,16,128]{3,2,1,0:T(8,128)(2,1)}, bf16[2,32,16,128]{3,2,1,0:T(8,128)(2,1)}, u32[]{:S(2)}, u32[]{:S(2)}) collective-permute-start(bf16[2,32,16,128]{3,2,1,0:T(8,128)(2,1)} %get-tuple-element.29.refs_0_), channel_id=1, source_target_pairs={{0,1},{1,0},{2,3},{3,2},{4,5},{5,4},{6,7},{7,6},{8,9},{9,8},{10,11... | collective-permute-start | bytes 786440 | tf_op jit(solution)/shard_map/ppermute | solution.py:53
  105.7 11.3 %collective-permute-start.18 = (bf16[2,32,16,128]{3,2,1,0:T(8,128)(2,1)S(1)}, bf16[2,32,16,128]{3,2,1,0:T(8,128)(2,1)}, u32[]{:S(2)}, u32[]{:S(2)}) collective-permute-start(bf16[2,32,16,128]{3,2,1,0:T(8,128)(2,1)S(1)} %collective-permute-done.14.refs_1_), channel_id=1, source_target_pairs={{0,1},{1,0},{2,3},{3,2},{4,5},{5,4},{6,7},{7,6},{8,9},{9,8},{10,11... | collective-permute-start | bytes 786440 | tf_op jit(solution)/shard_map/ppermute | solution.py:53
  110.2 6.8 %collective-permute-start.19 = (bf16[2,32,16,128]{3,2,1,0:T(8,128)(2,1)}, bf16[2,32,16,128]{3,2,1,0:T(8,128)(2,1)}, u32[]{:S(2)}, u32[]{:S(2)}) collective-permute-start(bf16[2,32,16,128]{3,2,1,0:T(8,128)(2,1)} %collective-permute-done.15.refs_2_), channel_id=1, source_target_pairs={{0,1},{1,0},{2,3},{3,2},{4,5},{5,4},{6,7},{7,6},{8,9},{9,8},{10,11... | collective-permute-start | bytes 786440 | tf_op jit(solution)/shard_map/ppermute | solution.py:53
  110.2 6.8 %collective-permute-start.20 = (bf16[2,32,16,128]{3,2,1,0:T(8,128)(2,1)}, bf16[2,32,16,128]{3,2,1,0:T(8,128)(2,1)}, u32[]{:S(2)}, u32[]{:S(2)}) collective-permute-start(bf16[2,32,16,128]{3,2,1,0:T(8,128)(2,1)} %collective-permute-done.16.refs_3_), channel_id=1, source_target_pairs={{0,1},{1,0},{2,3},{3,2},{4,5},{5,4},{6,7},{7,6},{8,9},{9,8},{10,11... | collective-permute-start | bytes 786440 | tf_op jit(solution)/shard_map/ppermute | solution.py:53
  (10 other events, 179.4 us)

commit v2 on v1

--- a/solution.py
+++ b/solution.py
@@ -59,29 +59,15 @@
     return (wide * lax.rsqrt(mean_sq + epsilon) * gain_row).astype(bf16)
 
 
-def side_by_side(ref):
-    return jnp.concatenate([ref[i] for i in range(ref.shape[0])], axis=1)
-
-
-def prepare_kernel(tokens, chosen, qw, ow, up, *outs):
-    bufs, (bundle, wanted, table, count) = outs[:-4], outs[-4:]
-    blocks = tokens.shape[0] // BLOCK
-    sl = BLOCK // (CHIPS * CORES)
-    owners = wanted.shape[0]
-    for buf, dx in zip(bufs, STEPS):
-        for core in range(CORES):
-            dest = CORES * chip_at(dx) + core
-            buf[core, 0] = tokens[pl.ds(pl.multiple_of(dest * BLOCK, BLOCK), BLOCK), :]
-            for b in range(blocks):
-                at = pl.multiple_of(b * BLOCK + dest * sl, sl)
-                buf[core, 1, b * sl : (b + 1) * sl, :] = tokens[pl.ds(at, sl), :]
-    at = qw.shape[0]
-    bundle[:at] = qw[...]
+def prepare_kernel(chosen, ow, up, bundle, wanted, table, count):
+    at = 0
     for c in range(0, ow.shape[1], LANES):
         bundle[at : at + ow.shape[0]] = ow[:, c : c + LANES]
         at += ow.shape[0]
     bundle[at:, : up.shape[2]] = up[0]
     bundle[at:, up.shape[2] :] = up[1]
+    blocks = chosen.shape[0]
+    owners = wanted.shape[0]
     mine = lax.axis_index(KV[0]) * lax.axis_size(KV[1]) + lax.axis_index(KV[1])
     c = chosen[...]
     valid = c >= 0
@@ -103,10 +89,20 @@
 
 
 def latent_kernel(asked, lw, *refs):
-    toks, (lat_out, send_out, tok) = refs[:-3], refs[-3:]
-    for part, source in zip(toks, SOURCES):
-        tok[came_from(source)] = part[lax.axis_index("core"), 1]
-    lat = jnp.dot(side_by_side(tok), lw[...], preferred_element_type=f32).astype(bf16)
+    n = len(SOURCES)
+    toks, (lat_out, send_out, tok, sem) = refs[:n], refs[n:]
+    mine = came_from((0, 0))
+    fetch = [
+        pltpu.make_async_copy(part.at[:, mine], tok.at[came_from(source)], sem.at[i])
+        for i, (part, source) in enumerate(zip(toks, SOURCES))
+    ]
+    for copy in fetch:
+        copy.start()
+    for copy in fetch:
+        copy.wait()
+    rows = lat_out.shape[0] * lat_out.shape[1]
+    lhs = jnp.concatenate([tok[i].reshape(rows, tok.shape[-1]) for i in range(n)], axis=1)
+    lat = jnp.dot(lhs, lw[...], preferred_element_type=f32).astype(bf16)
     lat_out[...] = lat.reshape(lat_out.shape)
     for o in range(send_out.shape[0]):
         for s in range(PER_OWNER):
@@ -125,39 +121,47 @@
                 out[core, c] = pool[table[dest, c]]
 
 
-def query_kernel(gain, *refs):
+def query_kernel(gain, qw, *refs):
     n = len(SOURCES)
-    toks, pieces, (out, tok, weights, sem) = refs[:n], refs[n : 2 * n], refs[2 * n :]
-    fetch = [
-        pltpu.make_async_copy(p.at[pl.ds(0, weights.shape[1])], weights.at[i], sem.at[i])
-        for i, p in enumerate(pieces)
-    ]
+    toks, outs, (tok, weights, sem) = refs[:n], refs[n:-3], refs[-3:]
+    feats = toks[0].shape[1]
+    fetch = [pltpu.make_async_copy(part, tok.at[i], sem.at[i]) for i, part in enumerate(toks)]
     for copy in fetch:
         copy.start()
-    for part, source in zip(toks, SOURCES):
-        tok[came_from(source)] = part[lax.axis_index("core"), 0]
-    lhs = side_by_side(tok)
+    for i, source in enumerate(SOURCES):
+        at = pl.multiple_of(came_from(source) * feats, feats)
+        weights[i * feats : (i + 1) * feats] = qw[pl.ds(at, feats), :]
+    for copy in fetch:
+        copy.wait()
     width = gain.shape[1]
-    heads = out.shape[0] // n
-    for i in range(n):
-        fetch[i].wait()
-        acc = jnp.dot(lhs, weights[i], preferred_element_type=f32).astype(bf16)
-        for h in range(heads):
-            out[i * heads + h] = normed(acc[:, h * width : (h + 1) * width], gain[...])
-
-
-def attend_kernel(count, q_ref, kgain, ogain, *refs):
+    for out, dx in zip(outs, STEPS):
+        for core in range(CORES):
+            dest = CORES * chip_at(dx) + core
+            rows = pl.ds(pl.multiple_of(dest * BLOCK, BLOCK), BLOCK)
+            lhs = jnp.concatenate([tok[i, rows, :] for i in range(n)], axis=1)
+            acc = jnp.dot(lhs, weights[...], preferred_element_type=f32).astype(bf16)
+            for h in range(out.shape[1]):
+                out[core, h] = normed(acc[:, h * width : (h + 1) * width], gain[...])
+
+
+def attend_kernel(count, kgain, ogain, *refs):
     n = len(SOURCES)
-    pieces, bundles, (out, kv, weights, acc, kv_sem, weight_sem) = refs[:n], refs[n : 2 * n], refs[2 * n :]
+    queries, pieces, bundles = refs[:n], refs[n : 2 * n], refs[2 * n : 3 * n]
+    out, q_ref, kv, weights, acc, q_sem, kv_sem, weight_sem = refs[3 * n :]
     mine = lax.axis_index("core")
+    each = queries[0].shape[1]
+    asked = [
+        pltpu.make_async_copy(p.at[mine], q_ref.at[pl.ds(i * each, each)], q_sem.at[i])
+        for i, p in enumerate(queries)
+    ]
     fetch = [pltpu.make_async_copy(p.at[mine], kv.at[i], kv_sem.at[i]) for i, p in enumerate(pieces)]
-    first = bundles[0].shape[0] - weights.shape[1]
     later = [
-        pltpu.make_async_copy(b.at[pl.ds(first, weights.shape[1])], weights.at[i], weight_sem.at[i])
-        for i, b in enumerate(bundles)
+        pltpu.make_async_copy(b, weights.at[i], weight_sem.at[i]) for i, b in enumerate(bundles)
     ]
-    for copy in fetch + later:
+    for copy in asked + fetch + later:
         copy.start()
+    for copy in asked:
+        copy.wait()
     _, picks, sl, width = kv.shape
     keys = picks * sl
     heads = q_ref.shape[0]
@@ -235,40 +239,54 @@
     owners = lax.axis_size(KV)
     tp = len(SOURCES)
     sl = BLOCK // tp
-    heads = query_weight.shape[1] // lat_w * tp
-    q_rows = query_weight.shape[0]
+    each = query_weight.shape[1] // lat_w
+    heads = each * tp
     late_rows = (out_weight.size + value_up.size) // LANES
 
-    *bufs, bundle, wanted, table, count = pl.pallas_call(
+    toks_x = over_x([tokens] * CHIPS)
+
+    bundle, wanted, table, count = pl.pallas_call(
         prepare_kernel,
-        out_shape=[shape((CORES, 2, BLOCK, feats))] * CHIPS
-        + [
-            shape((q_rows + late_rows, LANES)),
+        out_shape=[
+            shape((late_rows, LANES)),
             shape((owners, 1, BLOCK), i32),
             shape((blocks, picks), i32),
             shape((blocks, BLOCK), i32),
         ],
-        in_specs=[VMEM] * 5,
-        out_specs=[VMEM] * (CHIPS + 4),
+        in_specs=[VMEM] * 3,
+        out_specs=[VMEM] * 4,
         name="prepare",
-    )(tokens, chosen, query_weight, out_weight, value_up.swapaxes(1, 2))
-
-    toks_x = over_x(bufs)
+    )(chosen, out_weight, value_up.swapaxes(1, 2))
+
+    asked = lax.all_to_all(wanted, KV, split_axis=0, concat_axis=0, tiled=True)
     bundles_x = over_x([bundle] * CHIPS)
-    asked = lax.all_to_all(wanted, KV, split_axis=0, concat_axis=0, tiled=True)
     toks = with_partner(toks_x)
 
     latent, send = pl.pallas_call(
         latent_kernel,
         out_shape=(shape((blocks, sl, lat_w)), shape((owners, PER_OWNER, sl, lat_w))),
-        in_specs=[SMEM] + [VMEM] * (tp + 1),
+        in_specs=[SMEM, VMEM] + [ANY] * tp,
         out_specs=(VMEM, VMEM),
-        scratch_shapes=[pltpu.VMEM((tp, BLOCK, feats), bf16)],
+        scratch_shapes=[pltpu.VMEM((tp, blocks, sl, feats), bf16), pltpu.SemaphoreType.DMA((tp,))],
         name="latent",
-    )(asked, latent_weight, *toks)
+    )(asked, latent_weight, *[t.reshape(blocks, tp, sl, feats) for t in toks])
 
     got = lax.all_to_all(send, KV, split_axis=0, concat_axis=0, tiled=True)
     got = got.reshape(owners * PER_OWNER, sl, lat_w)
+
+    queries = pl.pallas_call(
+        query_kernel,
+        out_shape=[shape((CORES, each, BLOCK, lat_w))] * CHIPS,
+        in_specs=[VMEM, VMEM] + [ANY] * tp,
+        out_specs=[VMEM] * CHIPS,
+        scratch_shapes=[
+            pltpu.VMEM((tp, rows, feats), bf16),
+            pltpu.VMEM((tp * feats, query_weight.shape[1]), bf16),
+            pltpu.SemaphoreType.DMA((tp,)),
+        ],
+        name="query",
+    )(query_gain[None, :], query_weight, *toks)
+    queries_x = over_x(queries)
 
     picked = pl.pallas_call(
         pick_kernel,
@@ -278,37 +296,28 @@
         scratch_shapes=[pltpu.VMEM((blocks + owners * PER_OWNER, sl, lat_w), bf16)],
         name="pick",
     )(table, latent, got)
-    kv = with_partner(over_x(picked))
+    picked_x = over_x(picked)
+    q = with_partner(queries_x)
     bundles = with_partner(bundles_x)
-
-    q = pl.pallas_call(
-        query_kernel,
-        out_shape=shape((heads, BLOCK, lat_w)),
-        in_specs=[VMEM] * (tp + 1) + [ANY] * tp,
-        out_specs=VMEM,
-        scratch_shapes=[
-            pltpu.VMEM((tp, BLOCK, feats), bf16),
-            pltpu.VMEM((tp, q_rows, LANES), bf16),
-            pltpu.SemaphoreType.DMA((tp,)),
-        ],
-        name="query",
-    )(query_gain[None, :], *toks, *bundles)
+    kv = with_partner(picked_x)
 
     width = out_weight.shape[1] // tp
     res = pl.pallas_call(
         attend_kernel,
         out_shape=shape((tp, BLOCK, width)),
-        in_specs=[SMEM] + [VMEM] * 3 + [ANY] * (2 * tp),
+        in_specs=[SMEM] + [VMEM] * 2 + [ANY] * (3 * tp),
         out_specs=VMEM,
         scratch_shapes=[
+            pltpu.VMEM((heads, BLOCK, lat_w), bf16),
             pltpu.VMEM((tp, picks, sl, lat_w), bf16),
             pltpu.VMEM((tp, late_rows, LANES), bf16),
             pltpu.VMEM((heads * BLOCK // ROWS, ROWS, 2 * lat_w), f32),
             pltpu.SemaphoreType.DMA((tp,)),
             pltpu.SemaphoreType.DMA((tp,)),
+            pltpu.SemaphoreType.DMA((tp,)),
         ],
         name="attend",
-    )(count, q, key_gain[None, :], out_gain[None, :], *kv, *bundles)
+    )(count, key_gain[None, :], out_gain[None, :], *q, *kv, *bundles)
 
     res = lax.all_to_all(res, TP, split_axis=0, concat_axis=0, tiled=True)
     return res.reshape(rows, width)

time: 145 us -> 117 us (0.81)
  the two profiles are of different devices: /device:TPU:1 before, /device:TPU:8 now
where the time goes in v2:
time: 117 us; the launch traced here: 115 us
  blocking collectives  32.5 us (28%)
  Pallas kernels  28 us (24%)
  starting transfers between devices  27.6 us (24%)
  waiting for transfers between devices  22.5 us (19%)
  local copies, waits for them, and re-layouts  3.73 us (3%)
    all_to_all x1, blocking collectives, shards(): asked = lax.all_to_all(wanted, KV, split_axis=0, concat_axis=0, tiled=True)  20.2 us
    ppermute x12, starting transfers between devices, over_x(): lax.ppermute(part, 'x', [(i, (i + dx) % CHIPS) for i in range(CHIPS)])  19.3 us
    ppermute x12, waiting for transfers between devices, over_x(): lax.ppermute(part, 'x', [(i, (i + dx) % CHIPS) for i in range(CHIPS)])  17 us
    pallas_call x1, Pallas kernels, shards(): pl.pallas_call(attend_kernel, out_shape=shape((tp, BLOCK, width)), in_spe...  16.8 us
    all_to_all x1, blocking collectives, shards(): res = lax.all_to_all(res, TP, split_axis=0, concat_axis=0, tiled=True)  12.3 us
    all_to_all x1, starting transfers between devices, shards(): got = lax.all_to_all(send, KV, split_axis=0, concat_axis=0, tiled=True)  5.27 us
    pallas_call x1, Pallas kernels, shards(): pl.pallas_call(query_kernel, out_shape=[shape((CORES, each, BLOCK, lat_w)...  4.14 us
    unnamed x65, local copies, waits for them, and re-layouts  3.73 us
  transfers between devices with their start and end apart: 29, of which 9 were waited for; matrix products, arithmetic and copies ran while one was open for 0% of the time, Pallas kernels for 10%

profile of v2, /device:TPU:8, one launch (start us, length us, event | category | flops | bytes accessed | tf_op | source)
XLA Modules:
  0.0 114.6 jit_solution(8075037393806969264)
XLA Ops:
  0.0 3.0 %collective-permute-start.2 = (bf16[1024,128]{1,0:T(8,128)(2,1)}, bf16[1024,128]{1,0:T(8,128)(2,1)S(1)}, u32[]{:S(2)}, u32[]{:S(2)}) collective-permute-start(bf16[1024,128]{1,0:T(8,128)(2,1)} %refs_0_.1), channel_id=1, source_target_pairs={{0,4},{2,6},{4,0},{6,2},{1,5},{3,7},{5,1},{7,3},{8,12},{10,14},{12... | collective-permute-start | bytes 786440 | tf_op jit(solution)/shard_map/ppermute | solution.py:48
  3.0 1.1 collective-permute-start.1
  4.2 0.9 collective-permute-start
  5.1 5.8 %collective-permute-done.2.refs_3_ = bf16[1024,128]{1,0:T(8,128)(2,1)S(1)} collective-permute-done((bf16[1024,128]{1,0:T(8,128)(2,1)}, bf16[1024,128]{1,0:T(8,128)(2,1)S(1)}, u32[]{:S(2)}, u32[]{:S(2)}) %collective-permute-start.2) | collective-permute-done | bytes 262176 | tf_op jit(solution)/shard_map/ppermute | solution.py:48
  10.9 4.6 %collective-permute-done.1.refs_2_ = bf16[1024,128]{1,0:T(8,128)(2,1)S(1)} collective-permute-done((bf16[1024,128]{1,0:T(8,128)(2,1)}, bf16[1024,128]{1,0:T(8,128)(2,1)S(1)}, u32[]{:S(2)}, u32[]{:S(2)}) %collective-permute-start.1) | collective-permute-done | bytes 262176 | tf_op jit(solution)/shard_map/ppermute | solution.py:48
  16.0 1.9 %prepare.1 = (bf16[576,256]{1,0:T(8,128)(2,1)}, s32[32,1,128]{2,1,0:T(1,128)}, s32[8,32]{1,0:T(8,128)}, s32[8,128]{1,0:T(8,128)}) custom-call(s32[8,32]{1,0:T(8,128)} %chosen.1, bf16[128,1024]{1,0:T(8,128)(2,1)} %ow.1, bf16[2,64,128]{2,1,0:T(8,128)(2,1)} %bitcast.24), custom_call_target="tpu_custom_call" | custom-call | tf_op jit(solution)/shard_map/prepare/pallas_call | solution.py:248
  18.0 2.5 %collective-permute-start.23 = (bf16[576,256]{1,0:T(8,128)(2,1)}, bf16[576,256]{1,0:T(8,128)(2,1)S(1)}, u32[]{:S(2)}, u32[]{:S(2)}) collective-permute-start(bf16[576,256]{1,0:T(8,128)(2,1)} %get-tuple-element.32.refs_16_), channel_id=1, source_target_pairs={{0,4},{2,6},{4,0},{6,2},{1,5},{3,7},{5,1},{7,3},{8,12},{10,14},{12... | collective-permute-start | bytes 884744 | tf_op jit(solution)/shard_map/ppermute | solution.py:48
  20.5 1.5 %collective-permute-start.22 = (bf16[576,256]{1,0:T(8,128)(2,1)}, bf16[576,256]{1,0:T(8,128)(2,1)S(1)}, u32[]{:S(2)}, u32[]{:S(2)}) collective-permute-start(bf16[576,256]{1,0:T(8,128)(2,1)} %get-tuple-element.32.refs_16_), channel_id=1, source_target_pairs={{0,6},{2,0},{4,2},{6,4},{1,7},{3,1},{5,3},{7,5},{8,14},{10,8},{12,... | collective-permute-start | bytes 884744 | tf_op jit(solution)/shard_map/ppermute | solution.py:48
  22.5 20.2 %all_to_all.15.asked = s32[32,1,128]{2,1,0:T(1,128)} all-to-all(s32[32,1,128]{2,1,0:T(1,128)} %get-tuple-element.25), channel_id=1, replica_groups=mesh['kv_0'=8,'kv_1'=4,'x'=4,'core'=2] {'kv_0','kv_1'}, dimensions={0} | all-to-all | bytes 32768 | tf_op jit(solution)/shard_map/all_to_all | solution.py:261
  43.5 2.9 %latent.1 = (bf16[8,16,128]{2,1,0:T(8,128)(2,1)}, bf16[32,2,16,128]{3,2,1,0:T(8,128)(2,1)}) custom-call(s32[32,1,128]{2,1,0:T(1,128)} %all_to_all.15.asked, bf16[1024,128]{1,0:T(8,128)(2,1)} %lw.1, bf16[8,8,16,128]{3,2,1,0:T(8,128)(2,1)} %bitcast.16, bf16[8,8,16,128]{3,2,1,0:T(8,128)(2,1)} %bitcast.19, bf16[8,8,16,128]{3,2,1,0:T(8,128)(2,1)} %bitcast.18, ...), custom_call_target="tpu_custom_call" | custom-call | tf_op jit(solution)/shard_map/latent/pallas_call | solution.py:265
  46.4 5.3 %all-to-all-start.1 = ((bf16[32,2,16,128]{3,2,1,0:T(8,128)(2,1)}), bf16[32,2,16,128]{3,2,1,0:T(8,128)(2,1)S(1)}, u32[]{:S(2)}, u32[]{:S(2)}) async-start(bf16[32,2,16,128]{3,2,1,0:T(8,128)(2,1)} %get-tuple-element.27), calls=%async_computation.1 | async-start | bytes 524288 | tf_op jit(solution)/shard_map/all_to_all | solution.py:274
  52.8 4.1 %query.1 = (bf16[2,2,128,128]{3,2,1,0:T(8,128)(2,1)}, bf16[2,2,128,128]{3,2,1,0:T(8,128)(2,1)}, bf16[2,2,128,128]{3,2,1,0:T(8,128)(2,1)}, bf16[2,2,128,128]{3,2,1,0:T(8,128)(2,1)}) custom-call(f32[1,128]{1,0:T(1,128)} %bitcast.27, bf16[1024,256]{1,0:T(8,128)(2,1)} %qw.1, bf16[1024,128]{1,0:T(8,128)(2,1)} %refs_0_.1, bf16[1024,128]{1,0:T(8,128)(2,1)} %copy-done.3, ...), custom_call_target="tpu_custom_call" | custom-call | tf_op jit(solution)/shard_map/query/pallas_call | solution.py:277
  57.0 1.2 %collective-permute-start.7 = (bf16[2,2,128,128]{3,2,1,0:T(8,128)(2,1)}, bf16[2,2,128,128]{3,2,1,0:T(8,128)(2,1)S(1)}, u32[]{:S(2)}, u32[]{:S(2)}) collective-permute-start(bf16[2,2,128,128]{3,2,1,0:T(8,128)(2,1)} %get-tuple-element.21), channel_id=1, source_target_pairs={{0,2},{2,4},{4,6},{6,0},{1,3},{3,5},{5,7},{7,1},{8,10},{10,12},{12... | collective-permute-start | bytes 393224 | tf_op jit(solution)/shard_map/ppermute | solution.py:48
  58.2 3.3 %all-to-all-done.1 = bf16[32,2,16,128]{3,2,1,0:T(8,128)(2,1)S(1)} async-done(((bf16[32,2,16,128]{3,2,1,0:T(8,128)(2,1)}), bf16[32,2,16,128]{3,2,1,0:T(8,128)(2,1)S(1)}, u32[]{:S(2)}, u32[]{:S(2)}) %all-to-all-start.1) | async-done | bytes 262176 | tf_op jit(solution)/shard_map/all_to_all | solution.py:274
  62.3 2.2 %pick.1 = (bf16[2,32,16,128]{3,2,1,0:T(8,128)(2,1)}, bf16[2,32,16,128]{3,2,1,0:T(8,128)(2,1)}, bf16[2,32,16,128]{3,2,1,0:T(8,128)(2,1)}, bf16[2,32,16,128]{3,2,1,0:T(8,128)(2,1)}) custom-call(s32[8,32]{1,0:T(8,128)} %get-tuple-element.24.table, bf16[8,16,128]{2,1,0:T(8,128)(2,1)} %get-tuple-element.26.own, bf16[64,16,128]{2,1,0:T(8,128)(2,1)} %bitcast.14), custom_call_target="tpu_custom_call" | custom-call | tf_op jit(solution)/shard_map/pick/pallas_call | solution.py:291
  64.5 2.8 %collective-permute-start.8 = (bf16[2,2,128,128]{3,2,1,0:T(8,128)(2,1)}, bf16[2,2,128,128]{3,2,1,0:T(8,128)(2,1)S(1)}, u32[]{:S(2)}, u32[]{:S(2)}) collective-permute-start(bf16[2,2,128,128]{3,2,1,0:T(8,128)(2,1)} %get-tuple-element.22), channel_id=1, source_target_pairs={{0,6},{2,0},{4,2},{6,4},{1,7},{3,1},{5,3},{7,5},{8,14},{10,8},{12,... | collective-permute-start | bytes 393224 | tf_op jit(solution)/shard_map/ppermute | solution.py:48
  68.3 2.6 %collective-permute-start.15 = (bf16[2,32,16,128]{3,2,1,0:T(8,128)(2,1)}, bf16[2,32,16,128]{3,2,1,0:T(8,128)(2,1)S(1)}, u32[]{:S(2)}, u32[]{:S(2)}) collective-permute-start(bf16[2,32,16,128]{3,2,1,0:T(8,128)(2,1)} %get-tuple-element.30), channel_id=1, source_target_pairs={{0,6},{2,0},{4,2},{6,4},{1,7},{3,1},{5,3},{7,5},{8,14},{10,8},{12,... | collective-permute-start | bytes 786440 | tf_op jit(solution)/shard_map/ppermute | solution.py:48
  71.0 2.0 %collective-permute-start.16 = (bf16[2,32,16,128]{3,2,1,0:T(8,128)(2,1)}, bf16[2,32,16,128]{3,2,1,0:T(8,128)(2,1)S(1)}, u32[]{:S(2)}, u32[]{:S(2)}) collective-permute-start(bf16[2,32,16,128]{3,2,1,0:T(8,128)(2,1)} %get-tuple-element.31), channel_id=1, source_target_pairs={{0,4},{2,6},{4,0},{6,2},{1,5},{3,7},{5,1},{7,3},{8,12},{10,14},{12... | collective-permute-start | bytes 786440 | tf_op jit(solution)/shard_map/ppermute | solution.py:48
  73.1 2.3 %collective-permute-done.9.refs_3_ = bf16[2,2,128,128]{3,2,1,0:T(8,128)(2,1)S(1)} collective-permute-done((bf16[2,2,128,128]{3,2,1,0:T(8,128)(2,1)S(1)}, bf16[2,2,128,128]{3,2,1,0:T(8,128)(2,1)S(1)}, u32[]{:S(2)}, u32[]{:S(2)}) %collective-permute-start.9) | collective-permute-done | bytes 131104 | tf_op jit(solution)/shard_map/ppermute | solution.py:48
  77.6 1.4 %collective-permute-done.14.refs_9_ = bf16[2,32,16,128]{3,2,1,0:T(8,128)(2,1)S(1)} collective-permute-done((bf16[2,32,16,128]{3,2,1,0:T(8,128)(2,1)}, bf16[2,32,16,128]{3,2,1,0:T(8,128)(2,1)S(1)}, u32[]{:S(2)}, u32[]{:S(2)}) %collective-permute-start.14) | collective-permute-done | bytes 262176 | tf_op jit(solution)/shard_map/ppermute | solution.py:48
  79.0 2.7 %collective-permute-done.15.refs_10_ = bf16[2,32,16,128]{3,2,1,0:T(8,128)(2,1)S(1)} collective-permute-done((bf16[2,32,16,128]{3,2,1,0:T(8,128)(2,1)}, bf16[2,32,16,128]{3,2,1,0:T(8,128)(2,1)S(1)}, u32[]{:S(2)}, u32[]{:S(2)}) %collective-permute-start.15) | collective-permute-done | bytes 262176 | tf_op jit(solution)/shard_map/ppermute | solution.py:48
  82.5 1.2 %collective-permute-done.13.refs_7_ = bf16[2,2,128,128]{3,2,1,0:T(8,128)(2,1)S(1)} collective-permute-done((bf16[2,2,128,128]{3,2,1,0:T(8,128)(2,1)S(1)}, bf16[2,2,128,128]{3,2,1,0:T(8,128)(2,1)S(1)}, u32[]{:S(2)}, u32[]{:S(2)}) %collective-permute-start.13) | collective-permute-done | bytes 131104 | tf_op jit(solution)/shard_map/ppermute | solution.py:53
  84.8 16.8 %attend.1 = bf16[8,128,128]{2,1,0:T(8,128)(2,1)} custom-call(s32[8,128]{1,0:T(8,128)} %get-tuple-element.19.count, f32[1,128]{1,0:T(1,128)} %bitcast.26, f32[1,1024]{1,0:T(1,128)} %bitcast.25, bf16[2,2,128,128]{3,2,1,0:T(8,128)(2,1)} %get-tuple-element.20.refs_0_, bf16[2,2,128,128]{3,2,1,0:T(8,128)(2,1)} %copy-done.24, bf16[2,2,128,128]{3,2,1,0:T(8,128)(2,1)} %copy-done.25, ...), custom_call_target="tpu_custom_call" | custom-call | tf_op jit(solution)/shard_map/attend/pallas_call | solution.py:305
  101.6 12.3 %all_to_all.16 = bf16[8,128,128]{2,1,0:T(8,128)(2,1)S(1)} all-to-all(bf16[8,128,128]{2,1,0:T(8,128)(2,1)} %attend.1), channel_id=1, replica_groups=mesh['kv_0'=8,'kv_1'=4,'x'=4,'core'=2] {'x','core'}, dimensions={0} | all-to-all | bytes 524288 | tf_op jit(solution)/shard_map/all_to_all | solution.py:322
  (106 shorter events, 9.2 us)
Async XLA Ops:
  0.0 10.9 %collective-permute-start.2 = (bf16[1024,128]{1,0:T(8,128)(2,1)}, bf16[1024,128]{1,0:T(8,128)(2,1)S(1)}, u32[]{:S(2)}, u32[]{:S(2)}) collective-permute-start(bf16[1024,128]{1,0:T(8,128)(2,1)} %refs_0_.1), channel_id=1, source_target_pairs={{0,4},{2,6},{4,0},{6,2},{1,5},{3,7},{5,1},{7,3},{8,12},{10,14},{12... | collective-permute-start | bytes 786440 | tf_op jit(solution)/shard_map/ppermute | solution.py:48
  3.0 12.5 %collective-permute-start.1 = (bf16[1024,128]{1,0:T(8,128)(2,1)}, bf16[1024,128]{1,0:T(8,128)(2,1)S(1)}, u32[]{:S(2)}, u32[]{:S(2)}) collective-permute-start(bf16[1024,128]{1,0:T(8,128)(2,1)} %refs_0_.1), channel_id=1, source_target_pairs={{0,6},{2,0},{4,2},{6,4},{1,7},{3,1},{5,3},{7,5},{8,14},{10,8},{12,... | collective-permute-start | bytes 786440 | tf_op jit(solution)/shard_map/ppermute | solution.py:48
  4.2 11.4 %collective-permute-start = (bf16[1024,128]{1,0:T(8,128)(2,1)}, bf16[1024,128]{1,0:T(8,128)(2,1)S(1)}, u32[]{:S(2)}, u32[]{:S(2)}) collective-permute-start(bf16[1024,128]{1,0:T(8,128)(2,1)} %refs_0_.1), channel_id=1, source_target_pairs={{0,2},{2,4},{4,6},{6,0},{1,3},{3,5},{5,7},{7,1},{8,10},{10,12},{12... | collective-permute-start | bytes 786440 | tf_op jit(solution)/shard_map/ppermute | solution.py:48
  5.1 15.4 %collective-permute-start.3 = (bf16[1024,128]{1,0:T(8,128)(2,1)}, bf16[1024,128]{1,0:T(8,128)(2,1)S(1)}, u32[]{:S(2)}, u32[]{:S(2)}) collective-permute-start(bf16[1024,128]{1,0:T(8,128)(2,1)} %refs_0_.1), channel_id=1, source_target_pairs={{0,1},{1,0},{2,3},{3,2},{4,5},{5,4},{6,7},{7,6},{8,9},{9,8},{10,11... | collective-permute-start | bytes 786440 | tf_op jit(solution)/shard_map/ppermute | solution.py:53
  10.9 11.1 %collective-permute-start.6 = (bf16[1024,128]{1,0:T(8,128)(2,1)S(1)}, bf16[1024,128]{1,0:T(8,128)(2,1)S(1)}, u32[]{:S(2)}, u32[]{:S(2)}) collective-permute-start(bf16[1024,128]{1,0:T(8,128)(2,1)S(1)} %collective-permute-done.2.refs_3_), channel_id=1, source_target_pairs={{0,1},{1,0},{2,3},{3,2},{4,5},{5,4},{6,7},{7,6},{8,9},{9,8},{10,11... | collective-permute-start | bytes 786440 | tf_op jit(solution)/shard_map/ppermute | solution.py:53
  15.5 27.2 %collective-permute-start.5 = (bf16[1024,128]{1,0:T(8,128)(2,1)S(1)}, bf16[1024,128]{1,0:T(8,128)(2,1)S(1)}, u32[]{:S(2)}, u32[]{:S(2)}) collective-permute-start(bf16[1024,128]{1,0:T(8,128)(2,1)S(1)} %collective-permute-done.1.refs_2_), channel_id=1, source_target_pairs={{0,1},{1,0},{2,3},{3,2},{4,5},{5,4},{6,7},{7,6},{8,9},{9,8},{10,11... | collective-permute-start | bytes 786440 | tf_op jit(solution)/shard_map/ppermute | solution.py:53
  15.5 27.2 %collective-permute-start.4 = (bf16[1024,128]{1,0:T(8,128)(2,1)S(1)}, bf16[1024,128]{1,0:T(8,128)(2,1)S(1)}, u32[]{:S(2)}, u32[]{:S(2)}) collective-permute-start(bf16[1024,128]{1,0:T(8,128)(2,1)S(1)} %collective-permute-done.refs_1_), channel_id=1, source_target_pairs={{0,1},{1,0},{2,3},{3,2},{4,5},{5,4},{6,7},{7,6},{8,9},{9,8},{10,11... | collective-permute-start | bytes 786440 | tf_op jit(solution)/shard_map/ppermute | solution.py:53
  18.0 33.8 %collective-permute-start.23 = (bf16[576,256]{1,0:T(8,128)(2,1)}, bf16[576,256]{1,0:T(8,128)(2,1)S(1)}, u32[]{:S(2)}, u32[]{:S(2)}) collective-permute-start(bf16[576,256]{1,0:T(8,128)(2,1)} %get-tuple-element.32.refs_16_), channel_id=1, source_target_pairs={{0,4},{2,6},{4,0},{6,2},{1,5},{3,7},{5,1},{7,3},{8,12},{10,14},{12... | collective-permute-start | bytes 884744 | tf_op jit(solution)/shard_map/ppermute | solution.py:48
  20.5 31.8 %collective-permute-start.22 = (bf16[576,256]{1,0:T(8,128)(2,1)}, bf16[576,256]{1,0:T(8,128)(2,1)S(1)}, u32[]{:S(2)}, u32[]{:S(2)}) collective-permute-start(bf16[576,256]{1,0:T(8,128)(2,1)} %get-tuple-element.32.refs_16_), channel_id=1, source_target_pairs={{0,6},{2,0},{4,2},{6,4},{1,7},{3,1},{5,3},{7,5},{8,14},{10,8},{12,... | collective-permute-start | bytes 884744 | tf_op jit(solution)/shard_map/ppermute | solution.py:48
  22.0 30.4 %collective-permute-start.21 = (bf16[576,256]{1,0:T(8,128)(2,1)}, bf16[576,256]{1,0:T(8,128)(2,1)S(1)}, u32[]{:S(2)}, u32[]{:S(2)}) collective-permute-start(bf16[576,256]{1,0:T(8,128)(2,1)} %get-tuple-element.32.refs_16_), channel_id=1, source_target_pairs={{0,2},{2,4},{4,6},{6,0},{1,3},{3,5},{5,7},{7,1},{8,10},{10,12},{12... | collective-permute-start | bytes 884744 | tf_op jit(solution)/shard_map/ppermute | solution.py:48
  46.4 15.2 %all-to-all-start.1 = ((bf16[32,2,16,128]{3,2,1,0:T(8,128)(2,1)}), bf16[32,2,16,128]{3,2,1,0:T(8,128)(2,1)S(1)}, u32[]{:S(2)}, u32[]{:S(2)}) async-start(bf16[32,2,16,128]{3,2,1,0:T(8,128)(2,1)} %get-tuple-element.27), calls=%async_computation.1 | async-start | bytes 524288 | tf_op jit(solution)/shard_map/all_to_all | solution.py:274
  51.7 12.8 %collective-permute-start.24 = (bf16[576,256]{1,0:T(8,128)(2,1)S(1)}, bf16[576,256]{1,0:T(8,128)(2,1)S(1)}, u32[]{:S(2)}, u32[]{:S(2)}) collective-permute-start(bf16[576,256]{1,0:T(8,128)(2,1)S(1)} %copy-done.8), channel_id=1, source_target_pairs={{0,1},{1,0},{2,3},{3,2},{4,5},{5,4},{6,7},{7,6},{8,9},{9,8},{10,11... | collective-permute-start | bytes 884744 | tf_op jit(solution)/shard_map/ppermute | solution.py:53
  51.8 15.5 %collective-permute-start.27 = (bf16[576,256]{1,0:T(8,128)(2,1)S(1)}, bf16[576,256]{1,0:T(8,128)(2,1)S(1)}, u32[]{:S(2)}, u32[]{:S(2)}) collective-permute-start(bf16[576,256]{1,0:T(8,128)(2,1)S(1)} %collective-permute-done.23.refs_19_), channel_id=1, source_target_pairs={{0,1},{1,0},{2,3},{3,2},{4,5},{5,4},{6,7},{7,6},{8,9},{9,8},{10,11... | collective-permute-start | bytes 884744 | tf_op jit(solution)/shard_map/ppermute | solution.py:53
  52.3 15.5 %collective-permute-start.26 = (bf16[576,256]{1,0:T(8,128)(2,1)S(1)}, bf16[576,256]{1,0:T(8,128)(2,1)S(1)}, u32[]{:S(2)}, u32[]{:S(2)}) collective-permute-start(bf16[576,256]{1,0:T(8,128)(2,1)S(1)} %collective-permute-done.22.refs_18_), channel_id=1, source_target_pairs={{0,1},{1,0},{2,3},{3,2},{4,5},{5,4},{6,7},{7,6},{8,9},{9,8},{10,11... | collective-permute-start | bytes 884744 | tf_op jit(solution)/shard_map/ppermute | solution.py:53
  52.4 15.9 %collective-permute-start.25 = (bf16[576,256]{1,0:T(8,128)(2,1)S(1)}, bf16[576,256]{1,0:T(8,128)(2,1)S(1)}, u32[]{:S(2)}, u32[]{:S(2)}) collective-permute-start(bf16[576,256]{1,0:T(8,128)(2,1)S(1)} %collective-permute-done.21.refs_17_), channel_id=1, source_target_pairs={{0,1},{1,0},{2,3},{3,2},{4,5},{5,4},{6,7},{7,6},{8,9},{9,8},{10,11... | collective-permute-start | bytes 884744 | tf_op jit(solution)/shard_map/ppermute | solution.py:53
  57.0 14.0 %collective-permute-start.7 = (bf16[2,2,128,128]{3,2,1,0:T(8,128)(2,1)}, bf16[2,2,128,128]{3,2,1,0:T(8,128)(2,1)S(1)}, u32[]{:S(2)}, u32[]{:S(2)}) collective-permute-start(bf16[2,2,128,128]{3,2,1,0:T(8,128)(2,1)} %get-tuple-element.21), channel_id=1, source_target_pairs={{0,2},{2,4},{4,6},{6,0},{1,3},{3,5},{5,7},{7,1},{8,10},{10,12},{12... | collective-permute-start | bytes 393224 | tf_op jit(solution)/shard_map/ppermute | solution.py:48
  64.5 8.5 %collective-permute-start.8 = (bf16[2,2,128,128]{3,2,1,0:T(8,128)(2,1)}, bf16[2,2,128,128]{3,2,1,0:T(8,128)(2,1)S(1)}, u32[]{:S(2)}, u32[]{:S(2)}) collective-permute-start(bf16[2,2,128,128]{3,2,1,0:T(8,128)(2,1)} %get-tuple-element.22), channel_id=1, source_target_pairs={{0,6},{2,0},{4,2},{6,4},{1,7},{3,1},{5,3},{7,5},{8,14},{10,8},{12,... | collective-permute-start | bytes 393224 | tf_op jit(solution)/shard_map/ppermute | solution.py:48
  67.4 8.1 %collective-permute-start.9 = (bf16[2,2,128,128]{3,2,1,0:T(8,128)(2,1)S(1)}, bf16[2,2,128,128]{3,2,1,0:T(8,128)(2,1)S(1)}, u32[]{:S(2)}, u32[]{:S(2)}) collective-permute-start(bf16[2,2,128,128]{3,2,1,0:T(8,128)(2,1)S(1)} %copy-done.31), channel_id=1, source_target_pairs={{0,4},{2,6},{4,0},{6,2},{1,5},{3,7},{5,1},{7,3},{8,12},{10,14},{12... | collective-permute-start | bytes 393224 | tf_op jit(solution)/shard_map/ppermute | solution.py:48
  67.8 11.2 %collective-permute-start.14 = (bf16[2,32,16,128]{3,2,1,0:T(8,128)(2,1)}, bf16[2,32,16,128]{3,2,1,0:T(8,128)(2,1)S(1)}, u32[]{:S(2)}, u32[]{:S(2)}) collective-permute-start(bf16[2,32,16,128]{3,2,1,0:T(8,128)(2,1)} %get-tuple-element.29), channel_id=1, source_target_pairs={{0,2},{2,4},{4,6},{6,0},{1,3},{3,5},{5,7},{7,1},{8,10},{10,12},{12... | collective-permute-start | bytes 786440 | tf_op jit(solution)/shard_map/ppermute | solution.py:48
  68.3 13.3 %collective-permute-start.15 = (bf16[2,32,16,128]{3,2,1,0:T(8,128)(2,1)}, bf16[2,32,16,128]{3,2,1,0:T(8,128)(2,1)S(1)}, u32[]{:S(2)}, u32[]{:S(2)}) collective-permute-start(bf16[2,32,16,128]{3,2,1,0:T(8,128)(2,1)} %get-tuple-element.30), channel_id=1, source_target_pairs={{0,6},{2,0},{4,2},{6,4},{1,7},{3,1},{5,3},{7,5},{8,14},{10,8},{12,... | collective-permute-start | bytes 786440 | tf_op jit(solution)/shard_map/ppermute | solution.py:48
  71.0 10.8 %collective-permute-start.16 = (bf16[2,32,16,128]{3,2,1,0:T(8,128)(2,1)}, bf16[2,32,16,128]{3,2,1,0:T(8,128)(2,1)S(1)}, u32[]{:S(2)}, u32[]{:S(2)}) collective-permute-start(bf16[2,32,16,128]{3,2,1,0:T(8,128)(2,1)} %get-tuple-element.31), channel_id=1, source_target_pairs={{0,4},{2,6},{4,0},{6,2},{1,5},{3,7},{5,1},{7,3},{8,12},{10,14},{12... | collective-permute-start | bytes 786440 | tf_op jit(solution)/shard_map/ppermute | solution.py:48
  75.4 6.7 %collective-permute-start.12 = (bf16[2,2,128,128]{3,2,1,0:T(8,128)(2,1)S(1)}, bf16[2,2,128,128]{3,2,1,0:T(8,128)(2,1)S(1)}, u32[]{:S(2)}, u32[]{:S(2)}) collective-permute-start(bf16[2,2,128,128]{3,2,1,0:T(8,128)(2,1)S(1)} %collective-permute-done.8.refs_2_), channel_id=1, source_target_pairs={{0,1},{1,0},{2,3},{3,2},{4,5},{5,4},{6,7},{7,6},{8,9},{9,8},{10,11... | collective-permute-start | bytes 393224 | tf_op jit(solution)/shard_map/ppermute | solution.py:53
  77.4 6.3 %collective-permute-start.17 = (bf16[2,32,16,128]{3,2,1,0:T(8,128)(2,1)}, bf16[2,32,16,128]{3,2,1,0:T(8,128)(2,1)S(1)}, u32[]{:S(2)}, u32[]{:S(2)}) collective-permute-start(bf16[2,32,16,128]{3,2,1,0:T(8,128)(2,1)} %get-tuple-element.28.refs_8_), channel_id=1, source_target_pairs={{0,1},{1,0},{2,3},{3,2},{4,5},{5,4},{6,7},{7,6},{8,9},{9,8},{10,11... | collective-permute-start | bytes 786440 | tf_op jit(solution)/shard_map/ppermute | solution.py:53
  79.0 4.8 %collective-permute-start.18 = (bf16[2,32,16,128]{3,2,1,0:T(8,128)(2,1)S(1)}, bf16[2,32,16,128]{3,2,1,0:T(8,128)(2,1)S(1)}, u32[]{:S(2)}, u32[]{:S(2)}) collective-permute-start(bf16[2,32,16,128]{3,2,1,0:T(8,128)(2,1)S(1)} %collective-permute-done.14.refs_9_), channel_id=1, source_target_pairs={{0,1},{1,0},{2,3},{3,2},{4,5},{5,4},{6,7},{7,6},{8,9},{9,8},{10,11... | collective-permute-start | bytes 786440 | tf_op jit(solution)/shard_map/ppermute | solution.py:53
  (37 other events, 298.5 us)
